TPU v7x, 256 devices: a whole 4x4x8 slice. The times are simulated.
256 devices in a mesh: sp: 32 (over z, y), tp: 8 (over x, core).
Axes of the slice: x: 4, y: 4, z: 8, core: 2. Of those that a mesh axis runs over, the one named last changes fastest.
Arguments:
- latent: bfloat16 [16384, 4096], P(('sp', 'tp')), may hold values from -3 to 3
- context: bfloat16 [1024, 4096], P('sp'), may hold values from -6 to 6
- cond: float32 [4096], replicated, may hold values from -6 to 6
- ctx_cond: float32 [4096], replicated, may hold values from -6 to 6
- w_shift: bfloat16 [4096, 4096], P('sp', 'tp'), may hold values from -0.1875 to 0.1875
- w_scale: bfloat16 [4096, 4096], P('sp', 'tp'), may hold values from -0.09375 to 0.15478516
- w_gate: bfloat16 [4096, 4096], P('sp', 'tp'), may hold values from -0.1875 to 0.1875
- w_query: bfloat16 [4096, 2048], P(None, 'tp'), may hold values from -0.09375 to 0.09375
- key_weight: bfloat16 [4096, 1024], P(None, 'tp'), may hold values from -0.09375 to 0.09375
- value_weight: bfloat16 [4096, 1024], P(None, 'tp'), may hold values from -0.09375 to 0.09375
- w_out: bfloat16 [2048, 4096], P('tp'), may hold values from -0.125 to 0.125
- sink: float32 [16], replicated, may hold values from 4 to 8
Outputs:
- mixed: bfloat16 [16384, 4096], P(('sp', 'tp'))
All inputs are finite; a program needn't handle non-finite values.
Results may differ from a plain program's by a relative error of at most 0.035.
Values may be sent and summed in bfloat16 or wider, within the bound.
A program may use at most 64 MiB of HBM per device.

v0:
```python
import jax
import jax.numpy as jnp
from jax import lax
from jax.sharding import PartitionSpec as P

HEAD_SIZE = 128
WINDOW_SIDE = 128
GRID_WIDTH = 64


EPS = 1e-05
THETA = 10000.0
MASKED = -1e30


def sent_to_all(value, axis):
    length = lax.axis_size(axis)
    return lax.all_to_all(
        jnp.broadcast_to(value[None], (length, *value.shape)), axis, 0, 0, tiled=True
    )


def taken_together(value, axis):
    everything = sent_to_all(value, axis)
    return jnp.sum(everything, axis=0)


def in_one(arrays, axis):
    line, at, done = (jnp.concatenate([a.reshape(-1) for a in arrays]), 0, [])
    subtotal = taken_together(line, axis)
    for a in arrays:
        done.append(subtotal[at : at + a.size].reshape(a.shape))
        at += a.size
    return tuple(done)


def side_by_side(arrays, axis, dim, along):
    widths = [a.shape[along] for a in arrays]
    both = jnp.concatenate(arrays, axis=along)
    filled = lax.all_gather(both, axis, axis=dim, tiled=True)
    return tuple(jnp.split(filled, [sum(widths[:k]) for k in range(1, len(widths))], axis=along))


def in_order(tiles, dim):
    tiles = jnp.moveaxis(tiles, 0, dim)
    lengths = tiles.shape
    return tiles.reshape(*lengths[:dim], lengths[dim] * lengths[dim + 1], *lengths[dim + 2 :])


def gather_directly(value, axis, dim):
    tiles = sent_to_all(value, axis)
    return in_order(tiles, dim)


def with_halo(cells, sides, width):
    for axis, dim in sides:
        count = lax.axis_size(axis)
        ends = count - 1
        head = lax.slice_in_dim(cells, 0, width, axis=dim)
        tail = lax.slice_in_dim(cells, cells.shape[dim] - width, cells.shape[dim], axis=dim)
        cells = jnp.concatenate(
            [
                lax.ppermute(tail, axis, [(i, (i + 1) % count) for i in range(ends)]),
                cells,
                lax.ppermute(head, axis, [((i + 1) % count, i) for i in range(ends)]),
            ],
            axis=dim,
        )
    return cells


def layer_norm(rows):
    values = rows.astype(jnp.float32)
    mean = jnp.mean(values, axis=-1, keepdims=True)
    var = jnp.mean(jnp.square(values - mean), axis=-1, keepdims=True)
    return (values - mean) * lax.rsqrt(var + EPS)


def rotate_half(values, token_position, width):
    half = width // 2
    inverse = THETA ** (-jnp.arange(half, dtype=jnp.float32) * 2.0 / width)
    angle = token_position.astype(jnp.float32)[:, None] * inverse[None, :]
    cosine = jnp.cos(angle)[:, None, :]
    sine = jnp.sin(angle)[:, None, :]
    first = values[..., :half]
    second = values[..., half:]
    return jnp.concatenate(
        [first * cosine - second * sine, second * cosine + first * sine], axis=-1
    )


def axial_rotation(heads, token_position, grid):
    width = heads.shape[-1] // 2
    values = heads.astype(jnp.float32)
    turned = jnp.concatenate(
        [
            rotate_half(values[..., :width], token_position // grid, width),
            rotate_half(values[..., width:], token_position % grid, width),
        ],
        axis=-1,
    )
    return turned.astype(jnp.bfloat16)


def sink_weights(scores, sink_column):
    top = jnp.maximum(jnp.max(scores, axis=-1, keepdims=True), sink_column)
    expo = jnp.exp(scores - top)
    return (expo / (jnp.sum(expo, axis=-1, keepdims=True) + jnp.exp(sink_column - top))).astype(
        jnp.bfloat16
    )


def shards(
    latent,
    context,
    cond,
    ctx_cond,
    w_shift,
    w_scale,
    w_gate,
    w_query,
    key_weight,
    value_weight,
    w_out,
    sink,
):
    sp_count = lax.axis_size("sp")
    sp_index = lax.axis_index("sp")
    tp_index = lax.axis_index("tp")
    block_rows = w_shift.shape[0]
    act = jax.nn.silu(jnp.stack([cond, ctx_cond])).astype(jnp.bfloat16)
    own_act = lax.dynamic_slice_in_dim(act, sp_index * block_rows, block_rows, 1)
    shift_part = jnp.dot(own_act, w_shift, preferred_element_type=jnp.float32)
    scale_part = jnp.dot(own_act, w_scale, preferred_element_type=jnp.float32)
    gate_part = jnp.dot(own_act[0:1], w_gate, preferred_element_type=jnp.float32)
    shift_sum, scale_sum, gate_sum = in_one((shift_part, scale_part, gate_part), "sp")
    shift, scale, gate = side_by_side((shift_sum, scale_sum, gate_sum), "tp", 1, 0)
    latent_mod = (layer_norm(latent) * (1.0 + scale[0]) + shift[0]).astype(jnp.bfloat16)
    ctx_mod = (layer_norm(context) * (1.0 + scale[1]) + shift[1]).astype(jnp.bfloat16)
    kv_cols = key_weight.shape[1]
    q_cols = w_query.shape[1]
    ctx_pair = gather_directly(
        jnp.concatenate(
            [
                jnp.dot(ctx_mod, key_weight, preferred_element_type=jnp.float32).astype(
                    jnp.bfloat16
                ),
                jnp.dot(ctx_mod, value_weight, preferred_element_type=jnp.float32).astype(
                    jnp.bfloat16
                ),
            ],
            axis=1,
        ),
        "sp",
        0,
    )
    piece = lax.all_gather(latent_mod, "tp", axis=0, tiled=True)
    projected_rows = jnp.concatenate(
        [
            jnp.dot(piece, w_query, preferred_element_type=jnp.float32).astype(jnp.bfloat16),
            jnp.dot(piece, key_weight, preferred_element_type=jnp.float32).astype(jnp.bfloat16),
            jnp.dot(piece, value_weight, preferred_element_type=jnp.float32).astype(jnp.bfloat16),
        ],
        axis=1,
    )
    tokens_here = projected_rows.shape[0]
    kv_heads = kv_cols // HEAD_SIZE
    q_heads = q_cols // HEAD_SIZE
    query_group = q_heads // kv_heads
    offset = sp_index * tokens_here
    token_position = offset + jnp.arange(tokens_here, dtype=jnp.int32)
    query = axial_rotation(
        projected_rows[:, :q_cols].reshape(tokens_here, q_heads, HEAD_SIZE),
        token_position,
        GRID_WIDTH,
    )
    key = axial_rotation(
        projected_rows[:, q_cols : q_cols + kv_cols].reshape(tokens_here, kv_heads, HEAD_SIZE),
        token_position,
        GRID_WIDTH,
    )
    value_rows = projected_rows[:, q_cols + kv_cols :]
    extended = with_halo(
        jnp.concatenate([key.reshape(tokens_here, kv_cols), value_rows], axis=1),
        (("sp", 0),),
        WINDOW_SIDE,
    )
    block_list = tokens_here // WINDOW_SIDE
    band = jnp.concatenate(
        [
            extended[shift_index * WINDOW_SIDE : shift_index * WINDOW_SIDE + tokens_here].reshape(
                block_list, WINDOW_SIDE, 2 * kv_cols
            )
            for shift_index in range(3)
        ],
        axis=1,
    )
    band_key = band[..., :kv_cols].reshape(block_list, 3 * WINDOW_SIDE, kv_heads, HEAD_SIZE)
    band_value = band[..., kv_cols:].reshape(block_list, 3 * WINDOW_SIDE, kv_heads, HEAD_SIZE)
    context_key_rows = ctx_pair[:, :kv_cols].reshape(-1, kv_heads, HEAD_SIZE)
    context_value_rows = ctx_pair[:, kv_cols:].reshape(-1, kv_heads, HEAD_SIZE)
    query_block_list = query.reshape(block_list, WINDOW_SIDE, kv_heads, query_group, HEAD_SIZE)
    factor = HEAD_SIZE ** (-0.5)
    band_scores = (
        jnp.einsum(
            "nqhgd,nkhd->nhgqk", query_block_list, band_key, preferred_element_type=jnp.float32
        )
        * factor
    )
    total = tokens_here * sp_count
    qpos = token_position.reshape(block_list, WINDOW_SIDE)[:, :, None]
    kpos = (
        offset
        - WINDOW_SIDE
        + (jnp.arange(block_list, dtype=jnp.int32) * WINDOW_SIDE)[:, None, None]
        + jnp.arange(3 * WINDOW_SIDE, dtype=jnp.int32)[None, None, :]
    )
    valid = (jnp.abs(kpos - qpos) <= WINDOW_SIDE) & (kpos >= 0) & (kpos < total)
    band_scores = jnp.where(valid[:, None, None], band_scores, MASKED)
    ctx_scores = (
        jnp.einsum(
            "nqhgd,khd->nhgqk",
            query_block_list,
            context_key_rows,
            preferred_element_type=jnp.float32,
        )
        * factor
    )
    own_sink = lax.dynamic_slice_in_dim(sink, tp_index * q_heads, q_heads).reshape(
        kv_heads, query_group
    )[:, :, None, None]
    weights = sink_weights(jnp.concatenate([band_scores, ctx_scores], axis=-1), own_sink)
    attended = jnp.einsum(
        "nhgqk,nkhd->nqhgd",
        weights[..., : 3 * WINDOW_SIDE],
        band_value,
        preferred_element_type=jnp.float32,
    ) + jnp.einsum(
        "nhgqk,khd->nqhgd",
        weights[..., 3 * WINDOW_SIDE :],
        context_value_rows,
        preferred_element_type=jnp.float32,
    )
    attended = attended.astype(jnp.bfloat16).reshape(tokens_here, q_cols)
    projected = lax.psum_scatter(
        jnp.dot(attended, w_out, preferred_element_type=jnp.float32).astype(jnp.bfloat16),
        "tp",
        scatter_dimension=0,
        tiled=True,
    ).astype(jnp.float32)
    return (latent.astype(jnp.float32) + gate[0][None, :] * projected).astype(jnp.bfloat16)


def solution(mesh):
    in_specs = (
        P(("sp", "tp"), None),
        P("sp", None),
        P(),
        P(),
        P("sp", "tp"),
        P("sp", "tp"),
        P("sp", "tp"),
        P(None, "tp"),
        P(None, "tp"),
        P(None, "tp"),
        P("tp", None),
        P(),
    )
    out_specs = P(("sp", "tp"), None)
    return jax.shard_map(shards, mesh=mesh, in_specs=in_specs, out_specs=out_specs, check_vma=False)
```

profile of v0, /device:TPU:1, one launch (start us, length us, event | category | flops | bytes accessed | tf_op | source)
XLA Modules:
  0.0 170.4 jit_solution(11445464485622171272)
XLA Ops:
  6.5 0.9 fusion.49
  7.4 1.1 fusion.50
  8.5 1.0 convolution_bitcast_fusion.1
  9.6 1.0 convolution_bitcast_fusion.2
  10.6 0.9 broadcast_in_dim.12
  11.5 12.1 %all-to-all-start = ((f32[32,1,2560]{2,1,0:T(1,128)}), f32[32,1,2560]{2,1,0:T(1,128)}, u32[]{:S(2)}, u32[]{:S(2)}) async-start(f32[32,1,2560]{2,1,0:T(1,128)} %broadcast_in_dim.12), calls=%async_computation | async-start | bytes 655360 | tf_op jit(solution)/shard_map/all_to_all | solution.py:18
  23.7 1.2 convert_reduce_fusion
  24.9 1.3 fusion.10
  26.3 10.1 %all-to-all-done = f32[32,1,2560]{2,1,0:T(1,128)} async-done(((f32[32,1,2560]{2,1,0:T(1,128)}), f32[32,1,2560]{2,1,0:T(1,128)}, u32[]{:S(2)}, u32[]{:S(2)}) %all-to-all-start) | async-done | bytes 327712 | tf_op jit(solution)/shard_map/all_to_all | solution.py:18
  36.4 1.2 reduce_sum.54
  37.6 15.3 %all_gather.6 = f32[5,4096]{1,0:T(8,128)S(1)} all-gather(f32[5,512]{1,0:T(8,128)S(1)} %pad_maximum_fusion.4), channel_id=1, replica_groups=mesh['sp'=32,'tp'=8] {'tp'}, dimensions={1}, use_global_device_ids=true | all-gather | bytes 92160 | tf_op jit(solution)/shard_map/all_gather | solution.py:40
  52.9 2.1 %fusion.13 = bf16[64,4096]{1,0:T(8,128)(2,1)} fusion(bf16[64,4096]{1,0:T(8,128)(2,1)} %param.12, f32[4096]{0:T(1024)S(1)} %bitcast.140, f32[4096]{0:T(1024)S(1)} %bitcast.141, f32[64]{0:T(128)S(1)} %add_rsqrt_fusion.1, f32[64]{0:T(128)S(1)} %broadcast_multiply_fusion.1), kind=kLoop, calls=%fused_computation.30 | loop fusion | flops 1572864 | bytes 1081856 | tf_op jit(solution)/shard_map/convert_element_type | solution.py:138
  55.1 0.6 dynamic_slice.7
  55.8 0.2 convert_reduce_fusion.1
  55.9 0.3 fusion.19
  56.3 1.9 %fusion.16 = pred[4,128,384]{1,2,0:T(8,128)(4,1)} fusion(s32[4,128]{1,0:T(4,128)S(1)} %add_add_fusion, s32[4,384]{1,0:T(4,128)S(1)} %iota_add_fusion, pred[4,384]{1,0:T(4,128)(4,1)S(1)} %get-tuple-element.33, pred[4,384]{1,0:T(4,128)(4,1)S(1)} %get-tuple-element.32), kind=kLoop, calls=%fused_computation.36 | loop fusion | flops 983040 | bytes 207872 | tf_op jit(solution)/shard_map/and | solution.py:218
  58.3 1.2 multiply_cosine_fusion.1
  59.5 1.5 convolution_convert_fusion.4
  61.0 0.3 convolution_convert_fusion.5
  61.4 0.9 broadcast_in_dim.15
  62.2 4.6 %all-to-all-start.1 = ((bf16[32,32,256]{2,1,0:T(8,128)(2,1)}), bf16[32,32,256]{2,1,0:T(8,128)(2,1)}, u32[]{:S(2)}, u32[]{:S(2)}) async-start(bf16[32,32,256]{2,1,0:T(8,128)(2,1)} %broadcast_in_dim.15), calls=%async_computation.1 | async-start | bytes 1048576 | tf_op jit(solution)/shard_map/all_to_all | solution.py:18
  66.9 17.7 %all-gather.2.cloned.1.call-done = bf16[512,4096]{1,0:T(8,128)(2,1)} async-done(((bf16[64,4096]{1,0:T(8,128)(2,1)}), bf16[512,4096]{1,0:T(8,128)(2,1)}) %all-gather.2.cloned.1.call-update) | async-done | bytes 4194320 | tf_op jit(solution)/shard_map/all_gather | solution.py:157
  84.6 3.7 %fusion.9 = f32[512,1,128]{0,2,1:T(8,128)S(1)} fusion(bf16[512,4096]{1,0:T(8,128)(2,1)} %all-gather.2.cloned.1.call-done, bf16[4096,128]{1,0:T(8,128)(2,1)S(1)} %copy-done.4), kind=kOutput, calls=%fused_computation.22 | convolution fusion | flops 537001984 | bytes 5505024 | tf_op jit(solution)/shard_map/dot_general | solution.py:161
  88.3 0.6 fusion.36
  89.6 3.7 %convolution_convert_fusion.2 = bf16[512,128]{1,0:T(8,128)(2,1)S(1)} fusion(bf16[512,4096]{1,0:T(8,128)(2,1)} %all-gather.2.cloned.1.call-done, bf16[4096,128]{1,0:T(8,128)(2,1)} %param.21), kind=kOutput, calls=%fused_computation.19 | convolution fusion | flops 536936448 | bytes 5373952 | tf_op jit(solution)/shard_map/dot_general | solution.py:162
  93.3 0.2 concatenate.88
  93.5 0.7 fusion.55
  94.2 3.7 %collective-permute-start = (bf16[128,256]{1,0:T(8,128)(2,1)}, bf16[128,256]{1,0:T(8,128)(2,1)}, u32[]{:S(2)}, u32[]{:S(2)}) collective-permute-start(bf16[128,256]{1,0:T(8,128)(2,1)} %get-tuple-element.19), channel_id=1, source_target_pairs={{0,8},{8,16},{16,24},{24,32},{32,40},{40,48},{48,56},{56,64},{64,7... | collective-permute-start | bytes 196616 | tf_op jit(solution)/shard_map/ppermute | solution.py:63
  97.9 1.6 collective-permute-start.1
  99.5 4.2 %convolution_convert_fusion.1 = bf16[512,256]{0,1:T(8,128)(2,1)S(1)} fusion(bf16[512,4096]{1,0:T(8,128)(2,1)} %all-gather.2.cloned.1.call-done, bf16[4096,256]{1,0:T(8,128)(2,1)} %param.19), kind=kOutput, calls=%fused_computation.17 | convolution fusion | flops 1073872896 | bytes 6553600 | tf_op jit(solution)/shard_map/dot_general | solution.py:160
  103.9 0.6 concatenate.98
  104.6 0.2 copy.70
  104.8 0.2 copy.71
  105.0 0.2 copy.69
  105.2 1.0 copy.68
  106.2 1.1 pad_maximum_fusion.3
  107.3 4.3 %fusion.59 = (f32[4,2,128]{2,1,0:T(2,128)}, f32[4,1,2,128,1024]{3,4,2,0,1:T(8,128)}) fusion(bf16[4,128,2,128]{3,1,2,0:T(8,128)(2,1)} %pad_maximum_fusion.3, bf16[1024,256]{1,0:T(8,128)(2,1)} %bitcast.31), kind=kOutput, calls=%fused_computation.123 | convolution fusion | flops 270531584 | bytes 4722688 | tf_op jit(solution)/shard_map/nqhgd,khd->nhgqk/dot_general | solution.py:221
  112.2 0.2 concatenate.95
  112.5 1.1 pad_maximum_fusion.2
  113.6 1.5 fusion.58
  115.2 0.8 fusion.1
  116.1 1.0 divide_convert_fusion
  117.0 0.4 convolution_bitcast_fusion
  117.4 1.4 fusion.7
  118.9 0.2 copy.76
  119.1 3.2 %convolution_convert_fusion = bf16[512,4096]{1,0:T(8,128)(2,1)} fusion(bf16[256,4096]{1,0:T(8,128)(2,1)S(1)} %copy-done, bf16[64,8,2,128]{3,2,1,0:T(2,128)(2,1)S(1)} %bitcast.122), kind=kOutput, calls=%fused_computation | convolution fusion | flops 1075838976 | bytes 6553600 | tf_op jit(solution)/shard_map/dot_general | solution.py:246
  122.3 39.3 %reduce-scatter.2.cloned.1.call-done = bf16[64,4096]{1,0:T(8,128)(2,1)} async-done(((bf16[512,4096]{1,0:T(8,128)(2,1)}), bf16[64,4096]{1,0:T(8,128)(2,1)}) %reduce-scatter.2.cloned.1.call-update) | async-done | bytes 524304 | tf_op jit(solution)/shard_map/reduce_scatter | solution.py:245
  161.6 2.0 %fusion.14 = bf16[64,4096]{1,0:T(8,128)(2,1)} fusion(bf16[64,4096]{1,0:T(8,128)(2,1)S(1)} %copy-done.2, bf16[64,4096]{1,0:T(8,128)(2,1)} %reduce-scatter.2.cloned.1.call-done, f32[4096]{0:T(1024)S(1)} %bitcast.139), kind=kLoop, calls=%fused_computation.31 | loop fusion | flops 1310720 | bytes 1589248 | tf_op jit(solution)/shard_map/convert_element_type | solution.py:251
  (85 shorter events, 2.0 us)
Async XLA Ops:
  6.5 112.5 %copy-start = (bf16[256,4096]{1,0:T(8,128)(2,1)S(1)}, bf16[256,4096]{1,0:T(8,128)(2,1)}, u32[]{:S(2)}) copy-start(bf16[256,4096]{1,0:T(8,128)(2,1)} %param.22) | copy-start | bytes 6291460
  6.5 48.5 %copy-start.20 = (f32[16]{0:T(128)S(1)}, f32[16]{0:T(128)}, u32[]{:S(2)}) copy-start(f32[16]{0:T(128)} %param.23) | copy-start | bytes 196
  6.5 49.2 %copy-start.3 = (bf16[32,4096]{1,0:T(8,128)(2,1)S(1)}, bf16[32,4096]{1,0:T(8,128)(2,1)}, u32[]{:S(2)}) copy-start(bf16[32,4096]{1,0:T(8,128)(2,1)} %param.13) | copy-start | bytes 786436
  6.5 54.5 %copy-start.4 = (bf16[4096,128]{1,0:T(8,128)(2,1)S(1)}, bf16[4096,128]{1,0:T(8,128)(2,1)}, u32[]{:S(2)}) copy-start(bf16[4096,128]{1,0:T(8,128)(2,1)} %param.20) | copy-start | bytes 3145732
  11.5 24.8 %all-to-all-start = ((f32[32,1,2560]{2,1,0:T(1,128)}), f32[32,1,2560]{2,1,0:T(1,128)}, u32[]{:S(2)}, u32[]{:S(2)}) async-start(f32[32,1,2560]{2,1,0:T(1,128)} %broadcast_in_dim.12), calls=%async_computation | async-start | bytes 655360 | tf_op jit(solution)/shard_map/all_to_all | solution.py:18
  23.7 61.0 %all-gather.2.cloned.1.call-start = ((), (), s32[]{:S(2)}) async-start(), calls=%async_computation.3 | async-start | bytes 4718592 | tf_op jit(solution)/shard_map/all_gather | solution.py:157
  62.2 45.1 %all-to-all-start.1 = ((bf16[32,32,256]{2,1,0:T(8,128)(2,1)}), bf16[32,32,256]{2,1,0:T(8,128)(2,1)}, u32[]{:S(2)}, u32[]{:S(2)}) async-start(bf16[32,32,256]{2,1,0:T(8,128)(2,1)} %broadcast_in_dim.15), calls=%async_computation.1 | async-start | bytes 1048576 | tf_op jit(solution)/shard_map/all_to_all | solution.py:18
  66.9 94.7 %reduce-scatter.2.cloned.1.call-start = ((), (), s32[]{:S(2)}) async-start(), calls=%async_computation.4 | async-start | bytes 4718592 | tf_op jit(solution)/shard_map/reduce_scatter | solution.py:245
  88.9 0.6 copy-start.6
  88.9 0.6 copy-start.8
  88.9 0.6 copy-start.10
  88.9 0.6 copy-start.12
  94.2 18.3 %collective-permute-start = (bf16[128,256]{1,0:T(8,128)(2,1)}, bf16[128,256]{1,0:T(8,128)(2,1)}, u32[]{:S(2)}, u32[]{:S(2)}) collective-permute-start(bf16[128,256]{1,0:T(8,128)(2,1)} %get-tuple-element.19), channel_id=1, source_target_pairs={{0,8},{8,16},{16,24},{24,32},{32,40},{40,48},{48,56},{56,64},{64,7... | collective-permute-start | bytes 196616 | tf_op jit(solution)/shard_map/ppermute | solution.py:63
  97.9 5.8 %copy-start.14 = (f32[512,32]{0,1:T(8,128)S(1)}, f32[512,32]{0,1:T(8,128)}, u32[]{:S(2)}) copy-start(f32[512,32]{0,1:T(8,128)} %get-tuple-element.28) | copy-start | bytes 196612
  97.9 5.9 %copy-start.15 = (f32[512,32]{0,1:T(8,128)S(1)}, f32[512,32]{0,1:T(8,128)}, u32[]{:S(2)}) copy-start(f32[512,32]{0,1:T(8,128)} %get-tuple-element.29) | copy-start | bytes 196612
  97.9 5.9 %copy-start.16 = (f32[512,32]{0,1:T(8,128)S(1)}, f32[512,32]{0,1:T(8,128)}, u32[]{:S(2)}) copy-start(f32[512,32]{0,1:T(8,128)} %get-tuple-element.34) | copy-start | bytes 196612
  97.9 5.9 %copy-start.17 = (f32[512,32]{0,1:T(8,128)S(1)}, f32[512,32]{0,1:T(8,128)}, u32[]{:S(2)}) copy-start(f32[512,32]{0,1:T(8,128)} %get-tuple-element.35) | copy-start | bytes 196612
  97.9 14.6 %collective-permute-start.1 = (bf16[128,256]{1,0:T(8,128)(2,1)}, bf16[128,256]{1,0:T(8,128)(2,1)}, u32[]{:S(2)}, u32[]{:S(2)}) collective-permute-start(bf16[128,256]{1,0:T(8,128)(2,1)} %get-tuple-element.20), channel_id=1, source_target_pairs={{8,0},{16,8},{24,16},{32,24},{40,32},{48,40},{56,48},{64,56},{72,6... | collective-permute-start | bytes 196616 | tf_op jit(solution)/shard_map/ppermute | solution.py:65
  107.3 4.4 %copy-start.13 = (bf16[512,1,32]{0,2,1:T(8,128)(2,1)S(1)}, bf16[512,1,32]{0,2,1:T(8,128)(2,1)}, u32[]{:S(2)}) copy-start(bf16[512,1,32]{0,2,1:T(8,128)(2,1)} %copy-done.12) | copy-start | bytes 98308
  107.3 4.5 %copy-start.11 = (bf16[512,1,32]{0,2,1:T(8,128)(2,1)S(1)}, bf16[512,1,32]{0,2,1:T(8,128)(2,1)}, u32[]{:S(2)}) copy-start(bf16[512,1,32]{0,2,1:T(8,128)(2,1)} %copy-done.10) | copy-start | bytes 98308
  107.3 4.6 %copy-start.9 = (bf16[512,1,32]{0,2,1:T(8,128)(2,1)S(1)}, bf16[512,1,32]{0,2,1:T(8,128)(2,1)}, u32[]{:S(2)}) copy-start(bf16[512,1,32]{0,2,1:T(8,128)(2,1)} %copy-done.8) | copy-start | bytes 98308
  107.3 4.8 %copy-start.7 = (bf16[512,1,32]{0,2,1:T(8,128)(2,1)S(1)}, bf16[512,1,32]{0,2,1:T(8,128)(2,1)}, u32[]{:S(2)}) copy-start(bf16[512,1,32]{0,2,1:T(8,128)(2,1)} %copy-done.6) | copy-start | bytes 98308
  107.3 6.3 %copy-start.5 = (bf16[4,128,2,128]{3,1,2,0:T(8,128)(2,1)S(1)}, bf16[4,128,2,128]{3,1,2,0:T(8,128)(2,1)}, u32[]{:S(2)}) copy-start(bf16[4,128,2,128]{3,1,2,0:T(8,128)(2,1)} %pad_maximum_fusion.3) | copy-start | bytes 786436
  112.5 2.7 %copy-start.18 = (f32[4,2,128]{2,1,0:T(2,128)S(1)}, f32[4,2,128]{2,1,0:T(2,128)}, u32[]{:S(2)}) copy-start(f32[4,2,128]{2,1,0:T(2,128)} %get-tuple-element.38) | copy-start | bytes 12292
  112.5 2.7 %copy-start.19 = (f32[2]{0:T(128)S(1)}, f32[2]{0:T(128)}, u32[]{:S(2)}) copy-start(f32[2]{0:T(128)} %dynamic_slice.7) | copy-start | bytes 28
  112.5 2.7 %copy-start.1 = (f32[4,1,2,128,1024]{3,4,2,0,1:T(8,128)S(1)}, f32[4,1,2,128,1024]{3,4,2,0,1:T(8,128)}, u32[]{:S(2)}) copy-start(f32[4,1,2,128,1024]{3,4,2,0,1:T(8,128)} %get-tuple-element.39) | copy-start | bytes 12582916
  119.0 42.5 %copy-start.2 = (bf16[64,4096]{1,0:T(8,128)(2,1)S(1)}, bf16[64,4096]{1,0:T(8,128)(2,1)}, u32[]{:S(2)}) copy-start(bf16[64,4096]{1,0:T(8,128)(2,1)} %param.12) | copy-start | bytes 1572868
Sparse Core Ops, SparseCore 0:
  55.2 29.4 all-gather.1
  122.4 39.0 reduce-scatter.1
where the time goes:
time: 173 us; the launch traced here: 170 us
  waiting for transfers between devices  67.1 us (39%)
  matrix products  27.4 us (16%)
  starting transfers between devices  22.1 us (13%)
  other arithmetic  17.3 us (10%)
  blocking collectives  15.3 us (9%)
  between operations  13.9 us (8%)
  local copies, waits for them, and re-layouts  7.21 us (4%)
    reduce_scatter x1, waiting for transfers between devices, shards(): lax.psum_scatter(jnp.dot(attended, w_out, preferred_element_type=jnp.floa...  39.3 us
    all_gather x1, waiting for transfers between devices, shards(): piece = lax.all_gather(latent_mod, 'tp', axis=0, tiled=True)  17.7 us
    all_to_all x2, starting transfers between devices, sent_to_all(): lax.all_to_all(jnp.broadcast_to(value[None], (length, *value.shape)), axi...  16.7 us
    all_gather x1, blocking collectives, side_by_side(): filled = lax.all_gather(both, axis, axis=dim, tiled=True)  15.3 us
    all_to_all x2, waiting for transfers between devices, sent_to_all(): lax.all_to_all(jnp.broadcast_to(value[None], (length, *value.shape)), axi...  10.1 us
    dot_general x1, matrix products, shards(): jnp.einsum('nqhgd,khd->nhgqk', query_block_list, context_key_rows, prefer...  4.34 us
    dot_general x1, matrix products, shards(): jnp.dot(piece, w_query, preferred_element_type=jnp.float32)  4.16 us
    dot_general x1, matrix products, shards(): jnp.dot(piece, value_weight, preferred_element_type=jnp.float32)  3.73 us
  transfers between devices with their start and end apart: 6, of which 3 were waited for; matrix products, arithmetic and copies ran while one was open for 19% of the time, Pallas kernels for 0%

commit v1 on v0

v1 whole, which is shorter than its diff:
```python
import jax
import jax.numpy as jnp
import numpy as np
from jax import lax
from jax.experimental import pallas as pl
from jax.experimental.pallas import tpu as pltpu
from jax.sharding import PartitionSpec as P

MESH = pl.DeviceIdType.MESH
F32 = jnp.float32
BF16 = jnp.bfloat16

NX, NY, NZ, NT = 4, 4, 8, 8
NSP = NY * NZ
HEAD = 128
SIDE = 128
BLOCK = 64
WIDTH = 4096
HALF = WIDTH // 2
PAIR = 2 * BLOCK
TOKENS = 16384
CTX_ROWS = 32
EPS = 1e-05
THETA = 10000.0
MASKED = -1e30
PIECES = 4
PIECE = HALF // PIECES


def kernel(
    latent, context, cond, ctx_cond, w_shift, w_scale, w_gate, wq, wk, wv, wo, sink, inverse, out,
    x_raw, x_mod, w_all, w_out, w_modulation, ctx_raw, ctx_mod, y_buf, z_buf, t_buf, mod_rows,
    product, query, kv, ckv, attended, partial, from_left, from_right, left_done, right_done,
    l_sem, ag_s, ag_r, w_s, w_r, y_s, y_r, z_s, z_r, t_s, t_r, cz_s, cz_r, cy_s, cy_r, cc_s, cc_r,
    kv_s, kv_r, h_s, h_r, o_s, o_r, d_s, d_r, c_s, c_r,
):
    sp = lax.axis_index("sp")
    tp = lax.axis_index("tp")
    z, y = sp // NY, sp % NY
    x, core = tp // 2, tp % 2
    sibling = x * 2 + 1 - core
    right, opposite, left = (x + 1) % NX, (x + 2) % NX, (x + 3) % NX
    sp_next, sp_back = (sp + 1) % NSP, (sp + NSP - 1) % NSP
    to_right, to_left = (sp, right * 2 + core), (sp, left * 2 + core)
    to_sibling = (sp, sibling)

    def remote(src, dst, send, recv, device):
        return pltpu.make_async_remote_copy(
            src_ref=src, dst_ref=dst, send_sem=send, recv_sem=recv, device_id=device, device_id_type=MESH
        )

    sent = []

    def send(*args):
        copy = remote(*args)
        copy.start()
        sent.append(copy)

    def received(dst, send_sem, recv_sem):
        remote(dst, dst, send_sem, recv_sem, to_sibling).wait_recv()

    local = [
        pltpu.make_async_copy(w_shift, w_modulation.at[0], l_sem.at[0]),
        pltpu.make_async_copy(w_scale, w_modulation.at[1], l_sem.at[1]),
        pltpu.make_async_copy(w_gate, w_modulation.at[2], l_sem.at[2]),
        pltpu.make_async_copy(latent, x_raw.at[x], l_sem.at[3]),
        pltpu.make_async_copy(context, ctx_raw, l_sem.at[4]),
        pltpu.make_async_copy(wq, w_all.at[core, :, 0:256], l_sem.at[5]),
        pltpu.make_async_copy(wk, w_all.at[core, :, 256:384], l_sem.at[6]),
        pltpu.make_async_copy(wv, w_all.at[core, :, 384:512], l_sem.at[7]),
        pltpu.make_async_copy(wo, w_out.at[core], l_sem.at[8]),
    ]
    for copy in local:
        copy.start()

    barrier = pltpu.get_barrier_semaphore()
    greeted = [(sp, (tp + d) % NT) for d in range(1, NT)]
    greeted += [(z * NY + (y + d) % NY, tp) for d in range(1, NY)]
    greeted += [(((z + d) % NZ) * NY + y, tp) for d in range(1, NZ)]
    greeted += [(sp_next, tp), (sp_next, sibling), (sp_back, tp), (sp_back, sibling)]
    for device in greeted:
        pl.semaphore_signal(barrier, inc=1, device_id=device, device_id_type=MESH)

    act = jnp.concatenate(
        [jax.nn.silu(cond[pl.ds(sp, 1), :]), jax.nn.silu(ctx_cond[pl.ds(sp, 1), :]), jnp.zeros((6, 128), F32)],
        axis=0,
    ).astype(BF16)
    y_buf[y] = jnp.zeros((24, 128), F32)
    for i in range(3):
        local[i].wait()
        part = jnp.dot(act, w_modulation[i], preferred_element_type=F32)
        for row in range(2 if i < 2 else 1):
            for c in range(4):
                at = (2 * i + row) * 4 + c
                y_buf[y, at : at + 1, :] = part[row : row + 1, c * 128 : (c + 1) * 128]

    pl.semaphore_wait(barrier, len(greeted))

    for d in range(1, NY):
        send(y_buf.at[y], y_buf.at[y], y_s.at[d - 1], y_r.at[d - 1], (z * NY + (y + d) % NY, tp))

    local[3].wait()
    first, second = pl.ds(0, BLOCK // 2), pl.ds(BLOCK // 2, BLOCK // 2)

    def gather(block, rows, i, device):
        send(x_raw.at[block, rows, :], x_raw.at[block, rows, :], ag_s.at[i], ag_r.at[i], device)

    gather(x, first, 0, to_right)
    gather(x, second, 1, to_left)
    gather(x, second, 2, to_right)
    gather(x, first, 3, to_left)

    send(wq, w_all.at[core, :, 0:256], w_s.at[0], w_r.at[0], to_sibling)
    send(wk, w_all.at[core, :, 256:384], w_s.at[1], w_r.at[1], to_sibling)
    send(wv, w_all.at[core, :, 384:512], w_s.at[2], w_r.at[2], to_sibling)
    send(wo, w_out.at[core], w_s.at[3], w_r.at[3], to_sibling)

    for d in range(1, NY):
        received(y_buf.at[(y + NY - d) % NY], y_s.at[d - 1], y_r.at[d - 1])
    z_buf[z] = jnp.sum(y_buf[...], axis=0)
    for d in (4, 3, 5, 2, 6, 1, 7):
        send(z_buf.at[z], z_buf.at[z], z_s.at[d - 1], z_r.at[d - 1], (((z + d) % NZ) * NY + y, tp))
    for d in range(1, NZ):
        received(z_buf.at[(z + NZ - d) % NZ], z_s.at[d - 1], z_r.at[d - 1])
    t_buf[tp] = jnp.sum(z_buf[...], axis=0)
    for d in range(1, NT):
        send(t_buf.at[tp], t_buf.at[tp], t_s.at[d - 1], t_r.at[d - 1], (sp, (tp + d) % NT))

    received(x_raw.at[left, first, :], ag_s.at[0], ag_r.at[0])
    gather(left, first, 4, to_right)
    received(x_raw.at[right, second, :], ag_s.at[1], ag_r.at[1])
    gather(right, second, 5, to_left)

    for d in range(1, NT):
        received(t_buf.at[(tp + NT - d) % NT], t_s.at[d - 1], t_r.at[d - 1])
    for t in range(NT):
        for row in range(5):
            for c in range(4):
                at = t * 512 + c * 128
                value = t_buf[t, row * 4 + c : row * 4 + c + 1, :]
                mod_rows[row : row + 1, at : at + 128] = 1.0 + value if row in (2, 3) else value

    def modulate(read, write, which):
        rows = read()
        values = rows.astype(F32)
        mean = jnp.mean(values, axis=-1, keepdims=True)
        centred = values - mean
        var = jnp.mean(jnp.square(centred), axis=-1, keepdims=True)
        normal = centred * lax.rsqrt(var + EPS)
        write((normal * mod_rows[2 + which : 3 + which, :] + mod_rows[which : which + 1, :]).astype(BF16))

    local[4].wait()

    @pl.loop(0, CTX_ROWS // 16)
    def _(i):
        at = pl.ds(pl.multiple_of(i * 16, 16), 16)

        def write(value):
            ctx_mod[at, :] = value

        modulate(lambda: ctx_raw[at, :], write, 1)

    for copy in local[5:9]:
        copy.wait()
    ckv[core, y, z] = jnp.dot(ctx_mod[...], w_all[core, :, 256:512], preferred_element_type=F32).astype(BF16)
    own = ckv.at[core, y, z]
    for d in (4, 3, 5, 2, 6, 1, 7):
        send(own, own, cz_s.at[d - 1], cz_r.at[d - 1], (((z + d) % NZ) * NY + y, tp))

    received(x_raw.at[left, second, :], ag_s.at[2], ag_r.at[2])
    received(x_raw.at[right, first, :], ag_s.at[3], ag_r.at[3])
    received(x_raw.at[opposite, first, :], ag_s.at[4], ag_r.at[4])
    received(x_raw.at[opposite, second, :], ag_s.at[5], ag_r.at[5])

    @pl.loop(0, NX * BLOCK // 16)
    def _(i):
        block = i // (BLOCK // 16)
        at = pl.ds(pl.multiple_of((i % (BLOCK // 16)) * 16, 16), 16)

        def write(value):
            x_mod[pl.ds(pl.multiple_of(i * 16, 16), 16), :] = value

        modulate(lambda: x_raw[block, at, :], write, 0)

    for d in range(1, NZ):
        received(ckv.at[core, y, (z + NZ - d) % NZ], cz_s.at[d - 1], cz_r.at[d - 1])
    line = ckv.at[core, y]
    for d in (2, 1, 3):
        send(line, line, cy_s.at[d - 1], cy_r.at[d - 1], (z * NY + (y + d) % NY, tp))
    send(line, line, cc_s.at[0], cc_r.at[0], to_sibling)

    other = w_all.at[1 - core]
    received(other.at[:, 0:256], w_s.at[0], w_r.at[0])
    received(other.at[:, 256:384], w_s.at[1], w_r.at[1])
    received(other.at[:, 384:512], w_s.at[2], w_r.at[2])

    @pl.loop(0, 2)
    def _(j):
        for c in range(2):
            product[j, c] = jnp.dot(
                x_mod[...], w_all[j, :, c * 256 : (c + 1) * 256], preferred_element_type=F32
            ).astype(BF16)

    lane = lax.broadcasted_iota(jnp.int32, (BLOCK, HEAD), 1)
    column = lax.broadcasted_iota(jnp.int32, (BLOCK, HEAD), 0)
    by_row = lane < HEAD // 2
    is_first = lane % (HEAD // 2) < HEAD // 4

    @pl.loop(0, NX)
    def _(b):
        grid_row = sp * NT + b * 2 + core
        position = jnp.where(by_row, grid_row, column).astype(F32)
        angle = position * inverse[0:1, :]
        cosine = jnp.cos(angle)
        sine = jnp.sin(angle)
        sine = jnp.where(is_first, -sine, sine)

        def turned(value):
            value = value.astype(F32)
            partner = jnp.where(is_first, pltpu.roll(value, 96, 1), pltpu.roll(value, 32, 1))
            return (value * cosine + partner * sine).astype(BF16)

        rows = pl.ds(pl.multiple_of(b * BLOCK, BLOCK), BLOCK)
        for j in range(2):
            for g in range(2):
                query[b, 2 * j + g] = turned(product[j, 0, rows, g * HEAD : (g + 1) * HEAD])
            kv[b + 1, core, :, j * HEAD : (j + 1) * HEAD] = turned(product[j, 1, rows, 0:HEAD])
            kv[b + 1, core, :, (2 + j) * HEAD : (3 + j) * HEAD] = product[j, 1, rows, HEAD : 2 * HEAD]

    for k, tp_there in enumerate((tp, sibling)):
        send(kv.at[NX, core], kv.at[0, core], h_s.at[k], h_r.at[k], (sp_next, tp_there))
        send(kv.at[1, core], kv.at[NX + 1, core], h_s.at[2 + k], h_r.at[2 + k], (sp_back, tp_there))
    for b in range(NX):
        send(kv.at[b + 1, core], kv.at[b + 1, core], kv_s.at[b], kv_r.at[b], to_sibling)

    for d in range(1, NY):
        line = ckv.at[core, (y + NY - d) % NY]
        received(line, cy_s.at[d - 1], cy_r.at[d - 1])
        send(line, line, cc_s.at[d], cc_r.at[d], to_sibling)

    for k, core_there in enumerate((core, 1 - core)):
        received(kv.at[0, core_there], h_s.at[k], h_r.at[k])
        received(kv.at[NX + 1, core_there], h_s.at[2 + k], h_r.at[2 + k])
    for b in range(NX):
        received(kv.at[b + 1, 1 - core], kv_s.at[b], kv_r.at[b])
    for d in range(NY):
        received(ckv.at[1 - core, (y + NY - d) % NY], cc_s.at[d], cc_r.at[d])

    factor = HEAD ** (-0.5)
    i_query = lax.broadcasted_iota(jnp.int32, (PAIR, 3 * PAIR), 0) % BLOCK + core * BLOCK
    i_key = lax.broadcasted_iota(jnp.int32, (PAIR, 3 * PAIR), 1) - PAIR
    near = jnp.abs(i_key - i_query) <= SIDE
    upper = lax.broadcasted_iota(jnp.int32, (PAIR, 1), 0) < BLOCK
    across = (((1,), (1,)), ((), ()))

    @pl.loop(0, NX)
    def _(b):
        place = i_key + (sp * NT * BLOCK + b * PAIR)
        valid = near & (place >= 0) & (place < TOKENS)
        for h in range(2):
            q = query[b, 2 * h : 2 * h + 2].reshape(PAIR, HEAD)
            k_band = kv[pl.ds(b, 3), :, :, h * HEAD : (h + 1) * HEAD].reshape(3 * PAIR, HEAD)
            v_band = kv[pl.ds(b, 3), :, :, (2 + h) * HEAD : (3 + h) * HEAD].reshape(3 * PAIR, HEAD)
            k_ctx = ckv[h, :, :, :, 0:HEAD].reshape(NSP * CTX_ROWS, HEAD)
            v_ctx = ckv[h, :, :, :, HEAD : 2 * HEAD].reshape(NSP * CTX_ROWS, HEAD)
            s_band = lax.dot_general(q, k_band, across, preferred_element_type=F32) * factor
            s_band = jnp.where(valid, s_band, MASKED)
            s_ctx = lax.dot_general(q, k_ctx, across, preferred_element_type=F32) * factor
            sinks = jnp.where(upper, sink[4 * x + 2 * h], sink[4 * x + 2 * h + 1])
            top = jnp.maximum(
                jnp.maximum(jnp.max(s_band, axis=-1, keepdims=True), jnp.max(s_ctx, axis=-1, keepdims=True)), sinks
            )
            e_band = jnp.exp(s_band - top)
            e_ctx = jnp.exp(s_ctx - top)
            total = (
                jnp.sum(e_band, axis=-1, keepdims=True)
                + jnp.sum(e_ctx, axis=-1, keepdims=True)
                + jnp.exp(sinks - top)
            )
            value = jnp.dot(e_band.astype(BF16), v_band, preferred_element_type=F32)
            value += jnp.dot(e_ctx.astype(BF16), v_ctx, preferred_element_type=F32)
            value = (value / total).astype(BF16)
            rows = pl.ds(pl.multiple_of(b * BLOCK, BLOCK), BLOCK)
            for g in range(2):
                attended[rows, (2 * h + g) * HEAD : (2 * h + g + 1) * HEAD] = value[g * BLOCK : (g + 1) * BLOCK]

    received(w_out.at[1 - core], w_s.at[3], w_r.at[3])
    for c in range(PIECES):
        for half in range(2):
            at = half * HALF + c * PIECE
            columns = slice(at, at + PIECE)
            result = jnp.dot(attended[:, 0:256], w_out[0, :, columns], preferred_element_type=F32)
            result += jnp.dot(attended[:, 256:512], w_out[1, :, columns], preferred_element_type=F32)
            result = result.astype(BF16)
            for b in range(NX):
                partial[b, :, columns] = result[b * BLOCK : (b + 1) * BLOCK]
        lower = pl.ds(c * PIECE, PIECE)
        higher = pl.ds(HALF + c * PIECE, PIECE)
        send(partial.at[opposite, :, lower], from_left.at[:, lower], o_s.at[0, c], o_r.at[0, c], to_right)
        send(partial.at[opposite, :, higher], from_right.at[:, lower], o_s.at[1, c], o_r.at[1, c], to_left)
    low, high = pl.ds(0, HALF), pl.ds(HALF, HALF)
    send(partial.at[right, :, high], left_done.at[:, high], d_s.at[0], d_r.at[0], to_right)
    send(partial.at[left, :, low], right_done.at[:, low], d_s.at[1], d_r.at[1], to_left)
    for c in range(PIECES):
        lower = pl.ds(c * PIECE, PIECE)
        higher = pl.ds(HALF + c * PIECE, PIECE)
        received(from_left.at[:, lower], o_s.at[0, c], o_r.at[0, c])
        partial[right, :, lower] = (partial[right, :, lower].astype(F32) + from_left[:, lower].astype(F32)).astype(BF16)
        send(partial.at[right, :, lower], left_done.at[:, lower], c_s.at[0, c], c_r.at[0, c], to_right)
        received(from_right.at[:, lower], o_s.at[1, c], o_r.at[1, c])
        partial[left, :, higher] = (partial[left, :, higher].astype(F32) + from_right[:, lower].astype(F32)).astype(BF16)
        send(partial.at[left, :, higher], right_done.at[:, higher], c_s.at[1, c], c_r.at[1, c], to_left)
    received(left_done.at[:, high], d_s.at[0], d_r.at[0])
    received(right_done.at[:, low], d_s.at[1], d_r.at[1])
    for c in range(PIECES):
        received(left_done.at[:, pl.ds(c * PIECE, PIECE)], c_s.at[0, c], c_r.at[0, c])
        received(right_done.at[:, pl.ds(HALF + c * PIECE, PIECE)], c_s.at[1, c], c_r.at[1, c])

    @pl.loop(0, BLOCK // 16)
    def _(i):
        at = pl.ds(pl.multiple_of(i * 16, 16), 16)
        projected = partial[x, at, :].astype(F32) + left_done[at, :].astype(F32) + right_done[at, :].astype(F32)
        out[at, :] = (x_raw[x, at, :].astype(F32) + mod_rows[4:5, :] * projected).astype(BF16)

    for copy in sent:
        copy.wait_send()


def shards(
    latent, context, cond, ctx_cond, w_shift, w_scale, w_gate, w_query, key_weight, value_weight, w_out, sink
):
    inverse = (THETA ** (-np.arange(HEAD // 4, dtype=np.float32) * np.float32(2.0) / np.float32(HEAD // 2))).astype(
        np.float32
    )
    inverse = jnp.asarray(np.tile(np.tile(inverse, 4)[None], (8, 1)))
    anywhere = pl.BlockSpec(memory_space=pl.ANY)
    inside = pl.BlockSpec(memory_space=pltpu.VMEM)
    dma = pltpu.SemaphoreType.DMA
    return pl.pallas_call(
        kernel,
        out_shape=jax.ShapeDtypeStruct((BLOCK, WIDTH), BF16),
        in_specs=[anywhere, anywhere, inside, inside]
        + [anywhere] * 7
        + [pl.BlockSpec(memory_space=pltpu.SMEM), inside],
        out_specs=inside,
        scratch_shapes=[
            pltpu.VMEM((NX, BLOCK, WIDTH), BF16),
            pltpu.VMEM((NX * BLOCK, WIDTH), BF16),
            pltpu.VMEM((2, WIDTH, 512), BF16),
            pltpu.VMEM((2, 256, WIDTH), BF16),
            pltpu.VMEM((3, 128, 512), BF16),
            pltpu.VMEM((CTX_ROWS, WIDTH), BF16),
            pltpu.VMEM((CTX_ROWS, WIDTH), BF16),
            pltpu.VMEM((NY, 24, 128), F32),
            pltpu.VMEM((NZ, 24, 128), F32),
            pltpu.VMEM((NT, 24, 128), F32),
            pltpu.VMEM((8, WIDTH), F32),
            pltpu.VMEM((2, 2, NX * BLOCK, 256), BF16),
            pltpu.VMEM((NX, 4, BLOCK, HEAD), BF16),
            pltpu.VMEM((NX + 2, 2, BLOCK, 512), BF16),
            pltpu.VMEM((2, NY, NZ, CTX_ROWS, 256), BF16),
            pltpu.VMEM((NX * BLOCK, 512), BF16),
            pltpu.VMEM((NX, BLOCK, WIDTH), BF16),
            pltpu.VMEM((BLOCK, HALF), BF16),
            pltpu.VMEM((BLOCK, HALF), BF16),
            pltpu.VMEM((BLOCK, WIDTH), BF16),
            pltpu.VMEM((BLOCK, WIDTH), BF16),
            dma((9,)), dma((6,)), dma((6,)), dma((4,)), dma((4,)),
            dma((3,)), dma((3,)), dma((7,)), dma((7,)), dma((7,)), dma((7,)),
            dma((7,)), dma((7,)), dma((3,)), dma((3,)), dma((4,)), dma((4,)),
            dma((4,)), dma((4,)), dma((4,)), dma((4,)),
            dma((2, PIECES)), dma((2, PIECES)), dma((2,)), dma((2,)), dma((2, PIECES)), dma((2, PIECES)),
        ],
        compiler_params=pltpu.CompilerParams(
            collective_id=0, has_side_effects=True, vmem_limit_bytes=60 * 1024 * 1024
        ),
    )(
        latent, context, cond.reshape(NSP, 128), ctx_cond.reshape(NSP, 128), w_shift, w_scale, w_gate,
        w_query, key_weight, value_weight, w_out, sink, inverse,
    )


def solution(mesh):
    in_specs = (
        P(("sp", "tp"), None), P("sp", None), P(), P(), P("sp", "tp"), P("sp", "tp"), P("sp", "tp"),
        P(None, "tp"), P(None, "tp"), P(None, "tp"), P("tp", None), P(),
    )
    out_specs = P(("sp", "tp"), None)
    return jax.shard_map(shards, mesh=mesh, in_specs=in_specs, out_specs=out_specs, check_vma=False)
```

time: 173 us -> 75.8 us (0.44); the launches traced: 170 us -> 75.6 us
  Pallas kernels: 0 us -> 73.7 us
  waiting for transfers between devices: 67.1 us -> 0 us
  matrix products: 27.4 us -> 0 us
  starting transfers between devices: 22.1 us -> 0 us
  other arithmetic: 17.3 us -> 0 us
  blocking collectives: 15.3 us -> 0 us
  between operations: 13.9 us -> 0.01 us
  local copies, waits for them, and re-layouts: 7.21 us -> 1.87 us
    pallas_call x0 -> x1, Pallas kernels: none -> 73.7 us  [shards(): pl.pallas_call(kernel, out_shape=jax.ShapeDtypeStruct((BLOCK, WIDTH), BF1...]
    reduce_scatter x1 -> x0, waiting for transfers between devices: 39.3 us -> none  [shards(): lax.psum_scatter(jnp.dot(attended, w_out, preferred_element_type=jnp.floa...]
    dot_general x13 -> x0, matrix products: 27.4 us -> none  [the longest x1 4.34 us: shards(): jnp.einsum('nqhgd,khd->nhgqk', query_block_list, context_key_rows, prefer...]
    all_gather x1 -> x0, waiting for transfers between devices: 17.7 us -> none  [shards(): piece = lax.all_gather(latent_mod, 'tp', axis=0, tiled=True)]
    all_to_all x2 -> x0, starting transfers between devices: 16.7 us -> none  [sent_to_all(): lax.all_to_all(jnp.broadcast_to(value[None], (length, *value.shape)), axi...]
    all_gather x1 -> x0, blocking collectives: 15.3 us -> none  [side_by_side(): filled = lax.all_gather(both, axis, axis=dim, tiled=True)]
    all_to_all x2 -> x0, waiting for transfers between devices: 10.1 us -> none  [sent_to_all(): lax.all_to_all(jnp.broadcast_to(value[None], (length, *value.shape)), axi...]
    convert_element_type x6 -> x0, other arithmetic: 6.02 us -> none  [the longest x1 2.09 us: shards(): (layer_norm(latent) * (1.0 + scale[0]) + shift[0]).astype(jnp.bfloat16)]
  transfers between devices with their start and end apart: 6 -> 0, of which waited for: 3 -> 0; matrix products, arithmetic and copies ran while one was open for 19% -> 0% of each run, Pallas kernels for 0% -> 0%
where the time goes in v1:
time: 75.8 us; the launch traced here: 75.6 us
  Pallas kernels  73.7 us (97%)
  local copies, waits for them, and re-layouts  1.87 us (2%)
    pallas_call x1, Pallas kernels, shards(): pl.pallas_call(kernel, out_shape=jax.ShapeDtypeStruct((BLOCK, WIDTH), BF1...  73.7 us
    unnamed x1, local copies, waits for them, and re-layouts  1.87 us

profile of v1, /device:TPU:1, one launch (start us, length us, event | category | flops | bytes accessed | tf_op | source)
XLA Modules:
  0.0 75.6 jit_solution(12296232897633885137)
XLA Ops:
  0.0 73.7 %shard_map.127 = bf16[64,4096]{1,0:T(8,128)(2,1)} custom-call(bf16[64,4096]{1,0:T(8,128)(2,1)} %latent.1, bf16[32,4096]{1,0:T(8,128)(2,1)} %context.1, f32[32,128]{1,0:T(8,128)} %bitcast.2, f32[32,128]{1,0:T(8,128)} %bitcast.3, bf16[128,512]{1,0:T(8,128)(2,1)} %w_shift.1, bf16[128,512]{1,0:T(8,128)(2,1)} %w_scale.1, bf16[128,512]{1,0:T(8,128)(2,1)} %w_gate.1, ...), custom_call_target="tpu_custom_call" | custom-call | tf_op jit(solution)/shard_map/pallas_call | solution.py:339
  73.7 1.9 %copy.15 = bf16[64,4096]{1,0:T(8,128)(2,1)} copy(bf16[64,4096]{1,0:T(8,128)(2,1)} %shard_map.127) | data formatting | bytes 1048576

commit v2 on v1

v2 whole, which is shorter than its diff:
```python
import jax
import jax.numpy as jnp
import numpy as np
from jax import lax
from jax.experimental import pallas as pl
from jax.experimental.pallas import tpu as pltpu
from jax.sharding import PartitionSpec as P

MESH = pl.DeviceIdType.MESH
F32 = jnp.float32
BF16 = jnp.bfloat16

NX, NY, NZ, NT = 4, 4, 8, 8
NSP = NY * NZ
HEAD = 128
SIDE = 128
BLOCK = 64
WIDTH = 4096
HALF = WIDTH // 2
PAIR = 2 * BLOCK
TOKENS = 16384
CTX_ROWS = 32
EPS = 1e-05
THETA = 10000.0
MASKED = -1e30
PIECES = 4
PIECE = HALF // PIECES
ROWS = 16


def kernel(
    latent, context, cond_in, ctx_cond_in, w_shift, w_scale, w_gate, wq, wk, wv, wo, sink_in, inverse_in, out,
    cond, ctx_cond, sink, inverse, cosines, sines, x_raw, means, scales, x_mod, w_all, w_out, w_modulation, ctx_raw, ctx_mod, y_buf, z_buf, t_buf, mod_rows,
    product, query, kv, ckv, attended, partial, from_left, from_right, left_done, right_done,
    l_sem, ag_s, ag_r, w_s, w_r, y_s, y_r, z_s, z_r, t_s, t_r, cz_s, cz_r, cy_s, cy_r, cc_s, cc_r,
    kv_s, kv_r, h_s, h_r, o_s, o_r, d_s, d_r, c_s, c_r,
):
    sp = lax.axis_index("sp")
    tp = lax.axis_index("tp")
    z, y = sp // NY, sp % NY
    x, core = tp // 2, tp % 2
    sibling = x * 2 + 1 - core
    right, opposite, left = (x + 1) % NX, (x + 2) % NX, (x + 3) % NX
    sp_next, sp_back = (sp + 1) % NSP, (sp + NSP - 1) % NSP
    to_right, to_left = (sp, right * 2 + core), (sp, left * 2 + core)
    to_sibling = (sp, sibling)

    def remote(src, dst, send, recv, device):
        return pltpu.make_async_remote_copy(
            src_ref=src, dst_ref=dst, send_sem=send, recv_sem=recv, device_id=device, device_id_type=MESH
        )

    sent = []

    def send(*args):
        copy = remote(*args)
        copy.start()
        sent.append(copy)

    def received(dst, send_sem, recv_sem):
        remote(dst, dst, send_sem, recv_sem, to_sibling).wait_recv()

    local = [
        pltpu.make_async_copy(latent, x_raw.at[x], l_sem.at[0]),
        pltpu.make_async_copy(cond_in, cond, l_sem.at[1]),
        pltpu.make_async_copy(ctx_cond_in, ctx_cond, l_sem.at[2]),
        pltpu.make_async_copy(w_shift, w_modulation.at[0], l_sem.at[3]),
        pltpu.make_async_copy(w_scale, w_modulation.at[1], l_sem.at[4]),
        pltpu.make_async_copy(w_gate, w_modulation.at[2], l_sem.at[5]),
        pltpu.make_async_copy(context, ctx_raw, l_sem.at[6]),
        pltpu.make_async_copy(sink_in, sink, l_sem.at[7]),
        pltpu.make_async_copy(inverse_in, inverse, l_sem.at[8]),
        pltpu.make_async_copy(wq, w_all.at[core, :, 0:256], l_sem.at[9]),
        pltpu.make_async_copy(wk, w_all.at[core, :, 256:384], l_sem.at[10]),
        pltpu.make_async_copy(wv, w_all.at[core, :, 384:512], l_sem.at[11]),
        pltpu.make_async_copy(wo, w_out.at[core], l_sem.at[12]),
    ]
    for copy in local[:6]:
        copy.start()

    barrier = pltpu.get_barrier_semaphore()
    greeted = [(sp, (tp + d) % NT) for d in range(1, NT)]
    greeted += [(z * NY + (y + d) % NY, tp) for d in range(1, NY)]
    greeted += [(((z + d) % NZ) * NY + y, tp) for d in range(1, NZ)]
    greeted += [(sp_next, tp), (sp_next, sibling), (sp_back, tp), (sp_back, sibling)]
    for device in greeted:
        pl.semaphore_signal(barrier, inc=1, device_id=device, device_id_type=MESH)

    local[1].wait()
    local[2].wait()
    act = jnp.concatenate(
        [jax.nn.silu(cond[pl.ds(sp, 1), :]), jax.nn.silu(ctx_cond[pl.ds(sp, 1), :]), jnp.zeros((6, 128), F32)],
        axis=0,
    ).astype(BF16)
    y_buf[y] = jnp.zeros((24, 128), F32)
    for i in range(3):
        local[3 + i].wait()
        part = jnp.dot(act, w_modulation[i], preferred_element_type=F32)
        for row in range(2 if i < 2 else 1):
            for c in range(4):
                at = (2 * i + row) * 4 + c
                y_buf[y, at : at + 1, :] = part[row : row + 1, c * 128 : (c + 1) * 128]

    pl.semaphore_wait(barrier, len(greeted))

    for d in range(1, NY):
        send(y_buf.at[y], y_buf.at[y], y_s.at[d - 1], y_r.at[d - 1], (z * NY + (y + d) % NY, tp))

    local[0].wait()

    def rows_of(piece):
        return pl.ds(piece * ROWS, ROWS)

    def gather(block, piece, i, device):
        ref = x_raw.at[block, rows_of(piece), :]
        send(ref, ref, ag_s.at[i], ag_r.at[i], device)

    def own_pieces(i):
        gather(x, i, i, to_right)
        gather(x, 3 - i, 6 + i, to_left)

    def gathered(i):
        near = i < 4
        if near:
            received(x_raw.at[left, rows_of(i), :], ag_s.at[i], ag_r.at[i])
            received(x_raw.at[right, rows_of(3 - i), :], ag_s.at[6 + i], ag_r.at[6 + i])
        else:
            received(x_raw.at[opposite, rows_of(i - 4), :], ag_s.at[i], ag_r.at[i])
            received(x_raw.at[opposite, rows_of(7 - i), :], ag_s.at[6 + i], ag_r.at[6 + i])

    def forward(i):
        gather(left, i, 4 + i, to_right)
        gather(right, 3 - i, 10 + i, to_left)

    own_pieces(0)
    own_pieces(1)

    for copy in local[6:]:
        copy.start()

    send(wq, w_all.at[core, :, 0:256], w_s.at[0], w_r.at[0], to_sibling)
    send(wk, w_all.at[core, :, 256:384], w_s.at[1], w_r.at[1], to_sibling)
    send(wv, w_all.at[core, :, 384:512], w_s.at[2], w_r.at[2], to_sibling)

    def moments(read, rows):
        chunks = [slice(i * 128, (i + 1) * 128) for i in range(WIDTH // 128)]
        mean = jnp.sum(sum(read(at).astype(F32) for at in chunks), axis=-1, keepdims=True) / WIDTH
        mean = jnp.broadcast_to(mean, (rows, 128))
        var = sum(jnp.square(read(at).astype(F32) - mean) for at in chunks)
        var = jnp.sum(var, axis=-1, keepdims=True) / WIDTH
        return mean, jnp.broadcast_to(lax.rsqrt(var + EPS), (rows, 128))

    def statistics(block, half):
        rows = slice(half * 32, half * 32 + 32)
        means[block, rows, :], scales[block, rows, :] = moments(lambda at: x_raw[block, rows, at], 32)

    @pl.loop(0, 2)
    def _(i):
        at = pl.ds(pl.multiple_of(i * 32, 32), 32)
        means[x, at, :], scales[x, at, :] = moments(lambda columns: x_raw[x, at, columns], 32)

    lane = lax.broadcasted_iota(jnp.int32, (BLOCK, HEAD), 1)
    column = lax.broadcasted_iota(jnp.int32, (BLOCK, HEAD), 0)
    by_row = lane < HEAD // 2
    is_first = lane % (HEAD // 2) < HEAD // 4

    local[7].wait()
    local[8].wait()

    @pl.loop(0, NX)
    def _(b):
        position = jnp.where(by_row, sp * NT + b * 2 + core, column).astype(F32)
        angle = position * inverse[0:1, :]
        cosines[b] = jnp.cos(angle)
        sine = jnp.sin(angle)
        sines[b] = jnp.where(is_first, -sine, sine)

    for d in range(1, NY):
        received(y_buf.at[(y + NY - d) % NY], y_s.at[d - 1], y_r.at[d - 1])
    z_buf[z] = jnp.sum(y_buf[...], axis=0)
    for d in (4, 3, 5, 2, 6, 1, 7):
        send(z_buf.at[z], z_buf.at[z], z_s.at[d - 1], z_r.at[d - 1], (((z + d) % NZ) * NY + y, tp))
    own_pieces(2)
    for d in range(1, NZ):
        received(z_buf.at[(z + NZ - d) % NZ], z_s.at[d - 1], z_r.at[d - 1])
    t_buf[tp] = jnp.sum(z_buf[...], axis=0)
    for d in (4, 5, 3, 2, 6, 7, 1):
        send(t_buf.at[tp], t_buf.at[tp], t_s.at[d - 1], t_r.at[d - 1], (sp, (tp + d) % NT))
    own_pieces(3)
    send(wo, w_out.at[core], w_s.at[3], w_r.at[3], to_sibling)

    for i in range(2):
        gathered(i)
        forward(i)

    statistics(left, 0)
    statistics(right, 1)
    local[6].wait()
    ctx_mean, ctx_scale = moments(lambda at: ctx_raw[:, at], CTX_ROWS)

    for d in range(1, NT):
        received(t_buf.at[(tp + NT - d) % NT], t_s.at[d - 1], t_r.at[d - 1])
    for t in range(NT):
        for row in range(5):
            for c in range(4):
                at = t * 512 + c * 128
                value = t_buf[t, row * 4 + c : row * 4 + c + 1, :]
                mod_rows[row : row + 1, at : at + 128] = 1.0 + value if row in (2, 3) else value

    for i in range(WIDTH // 128):
        at = slice(i * 128, (i + 1) * 128)
        normal = (ctx_raw[:, at].astype(F32) - ctx_mean) * ctx_scale
        ctx_mod[:, at] = (normal * mod_rows[3:4, at] + mod_rows[1:2, at]).astype(BF16)
    for copy in local[9:]:
        copy.wait()
    halves = [
        jnp.dot(ctx_mod[:, at], w_all[core, at, 256:512], preferred_element_type=F32)
        for at in (slice(0, HALF), slice(HALF, WIDTH))
    ]
    ckv[core, y, z] = (halves[0] + halves[1]).astype(BF16)

    def spread(d):
        line = ckv.at[core, y, (z + NZ - d) % NZ]
        if d:
            received(line, cz_s.at[d - 1], cz_r.at[d - 1])
        for e in (2, 1, 3):
            send(line, line, cy_s.at[d, e - 1], cy_r.at[d, e - 1], (z * NY + (y + e) % NY, tp))
        send(line, line, cc_s.at[d, 0], cc_r.at[d, 0], to_sibling)

    def relay(d):
        for e in range(1, NY):
            line = ckv.at[core, (y + NY - e) % NY, (z + NZ - d) % NZ]
            received(line, cy_s.at[d, e - 1], cy_r.at[d, e - 1])
            send(line, line, cc_s.at[d, e], cc_r.at[d, e], to_sibling)

    own = ckv.at[core, y, z]
    for d in (4, 3, 5, 2, 6, 1, 7):
        send(own, own, cz_s.at[d - 1], cz_r.at[d - 1], (((z + d) % NZ) * NY + y, tp))
    spread(0)

    blocks = (x, right, left, opposite)

    def modulate(slot):
        block = blocks[slot]

        @pl.loop(0, WIDTH // 512)
        def _(c):
            for q in range(4):
                at = pl.ds(pl.multiple_of(c * 512 + q * 128, 128), 128)
                normal = (x_raw[block, :, at].astype(F32) - means[block]) * scales[block]
                x_mod[slot * BLOCK : (slot + 1) * BLOCK, at] = (
                    normal * mod_rows[2:3, at] + mod_rows[0:1, at]
                ).astype(BF16)

    modulate(0)
    gathered(2)
    gathered(3)

    statistics(left, 1)
    statistics(right, 0)

    modulate(1)
    modulate(2)

    def project(c, slot, slots):
        rows = slice(slot * BLOCK, (slot + slots) * BLOCK)
        for j in range(2):
            product[j, c, rows, :] = jnp.dot(
                x_mod[rows, :], w_all[j, :, c * 256 : (c + 1) * 256], preferred_element_type=F32
            ).astype(BF16)

    def place(slot):
        return (x + slot + slot // 2 * (5 - 2 * slot)) % NX, pl.ds(pl.multiple_of(slot * BLOCK, BLOCK), BLOCK)

    def turned(value, b):
        value = value.astype(F32)
        partner = jnp.where(is_first, pltpu.roll(value, 96, 1), pltpu.roll(value, 32, 1))
        return (value * cosines[b] + partner * sines[b]).astype(BF16)

    def turn_keys(slot):
        b, rows = place(slot)
        for j in range(2):
            kv[b + 1, core, :, j * HEAD : (j + 1) * HEAD] = turned(product[j, 1, rows, 0:HEAD], b)
            kv[b + 1, core, :, (2 + j) * HEAD : (3 + j) * HEAD] = product[j, 1, rows, HEAD : 2 * HEAD]

    def turn_queries(slot):
        b, rows = place(slot)
        for j in range(2):
            for g in range(2):
                query[b, 2 * j + g] = turned(product[j, 0, rows, g * HEAD : (g + 1) * HEAD], b)

    def share(slot):
        ref = kv.at[blocks[slot] + 1, core]
        send(ref, ref, kv_s.at[slot], kv_r.at[slot], to_sibling)

    halo = []
    for k, tp_there in enumerate((tp, sibling)):
        halo.append(remote(kv.at[NX, core], kv.at[0, core], h_s.at[k], h_r.at[k], (sp_next, tp_there)))
    for k, tp_there in enumerate((tp, sibling)):
        halo.append(remote(kv.at[1, core], kv.at[NX + 1, core], h_s.at[2 + k], h_r.at[2 + k], (sp_back, tp_there)))
    sent.extend(halo)

    def halo_when(last_late, first_late):
        @pl.when(last_late)
        def _():
            halo[0].start()
            halo[1].start()

        @pl.when(first_late)
        def _():
            halo[2].start()
            halo[3].start()

    other = w_all.at[1 - core]
    received(other.at[:, 0:256], w_s.at[0], w_r.at[0])
    received(other.at[:, 256:384], w_s.at[1], w_r.at[1])
    received(other.at[:, 384:512], w_s.at[2], w_r.at[2])
    project(1, 0, 3)
    for d in (1, 7, 2, 6):
        spread(d)

    @pl.loop(0, 3)
    def _(slot):
        turn_keys(slot)

    for slot in range(3):
        share(slot)
    halo_when(opposite != NX - 1, opposite != 0)
    project(0, 0, 3)
    for d in (3, 5, 4):
        spread(d)

    @pl.loop(0, 3)
    def _(slot):
        turn_queries(slot)

    gathered(4)
    gathered(5)

    statistics(opposite, 0)
    statistics(opposite, 1)
    modulate(3)
    project(1, 3, 1)
    turn_keys(3)
    share(3)
    halo_when(opposite == NX - 1, opposite == 0)
    for d in (0, 1, 7):
        relay(d)
    project(0, 3, 1)
    turn_queries(3)
    for d in (2, 6, 3, 5, 4):
        relay(d)
    for slot in (0, 1, 2, 3):
        received(kv.at[blocks[slot] + 1, 1 - core], kv_s.at[slot], kv_r.at[slot])
    for d in range(NZ):
        for e in range(NY):
            received(ckv.at[1 - core, (y + NY - e) % NY, (z + NZ - d) % NZ], cc_s.at[d, e], cc_r.at[d, e])
    for k, core_there in enumerate((core, 1 - core)):
        received(kv.at[0, core_there], h_s.at[k], h_r.at[k])
        received(kv.at[NX + 1, core_there], h_s.at[2 + k], h_r.at[2 + k])

    factor = HEAD ** (-0.5)
    i_query = lax.broadcasted_iota(jnp.int32, (PAIR, 3 * PAIR), 0) % BLOCK + core * BLOCK
    i_key = lax.broadcasted_iota(jnp.int32, (PAIR, 3 * PAIR), 1) - PAIR
    near = jnp.abs(i_key - i_query) <= SIDE
    upper = lax.broadcasted_iota(jnp.int32, (PAIR, 1), 0) < BLOCK
    across = (((1,), (1,)), ((), ()))

    def attend(b, slot):
        key_at = i_key + (sp * NT * BLOCK + b * PAIR)
        valid = near & (key_at >= 0) & (key_at < TOKENS)
        for h in range(2):
            q = query[b, 2 * h : 2 * h + 2].reshape(PAIR, HEAD)
            k_band = kv[pl.ds(b, 3), :, :, h * HEAD : (h + 1) * HEAD].reshape(3 * PAIR, HEAD)
            v_band = kv[pl.ds(b, 3), :, :, (2 + h) * HEAD : (3 + h) * HEAD].reshape(3 * PAIR, HEAD)
            k_ctx = ckv[h, :, :, :, 0:HEAD].reshape(NSP * CTX_ROWS, HEAD)
            v_ctx = ckv[h, :, :, :, HEAD : 2 * HEAD].reshape(NSP * CTX_ROWS, HEAD)
            s_band = lax.dot_general(q, k_band, across, preferred_element_type=F32) * factor
            s_band = jnp.where(valid, s_band, MASKED)
            s_ctx = lax.dot_general(q, k_ctx, across, preferred_element_type=F32) * factor
            sinks = jnp.where(upper, sink[4 * x + 2 * h], sink[4 * x + 2 * h + 1])
            top = jnp.maximum(
                jnp.maximum(jnp.max(s_band, axis=-1, keepdims=True), jnp.max(s_ctx, axis=-1, keepdims=True)), sinks
            )
            e_band = jnp.exp(s_band - top)
            e_ctx = jnp.exp(s_ctx - top)
            total = (
                jnp.sum(e_band, axis=-1, keepdims=True)
                + jnp.sum(e_ctx, axis=-1, keepdims=True)
                + jnp.exp(sinks - top)
            )
            value = jnp.dot(e_band.astype(BF16), v_band, preferred_element_type=F32)
            value += jnp.dot(e_ctx.astype(BF16), v_ctx, preferred_element_type=F32)
            value = (value / total).astype(BF16)
            rows = slice(slot * BLOCK, (slot + 1) * BLOCK)
            for g in range(2):
                attended[rows, (2 * h + g) * HEAD : (2 * h + g + 1) * HEAD] = value[g * BLOCK : (g + 1) * BLOCK]

    def output(slot, slots, at, width):
        rows = slice(slot * BLOCK, (slot + slots) * BLOCK)
        columns = slice(at, at + width)
        result = jnp.dot(attended[rows, 0:256], w_out[0, :, columns], preferred_element_type=F32)
        result += jnp.dot(attended[rows, 256:512], w_out[1, :, columns], preferred_element_type=F32)
        result = result.astype(BF16)
        for s in range(slots):
            partial[slot + s, :, columns] = result[s * BLOCK : (s + 1) * BLOCK]

    attend(opposite, 3)
    received(w_out.at[1 - core], w_s.at[3], w_r.at[3])
    for c in range(PIECES):
        output(3, 1, c * PIECE, PIECE)
        output(3, 1, HALF + c * PIECE, PIECE)
        lower = pl.ds(c * PIECE, PIECE)
        higher = pl.ds(HALF + c * PIECE, PIECE)
        send(partial.at[3, :, lower], from_left.at[:, lower], o_s.at[0, c], o_r.at[0, c], to_right)
        send(partial.at[3, :, higher], from_right.at[:, lower], o_s.at[1, c], o_r.at[1, c], to_left)
    attend(right, 1)
    attend(left, 2)
    for c in range(2 * PIECES):
        output(1, 2, c * PIECE, PIECE)
    low, high = pl.ds(0, HALF), pl.ds(HALF, HALF)
    send(partial.at[1, :, high], left_done.at[:, high], d_s.at[0], d_r.at[0], to_right)
    send(partial.at[2, :, low], right_done.at[:, low], d_s.at[1], d_r.at[1], to_left)
    for c in range(PIECES):
        lower = pl.ds(c * PIECE, PIECE)
        higher = pl.ds(HALF + c * PIECE, PIECE)
        received(from_left.at[:, lower], o_s.at[0, c], o_r.at[0, c])
        partial[1, :, lower] = (partial[1, :, lower].astype(F32) + from_left[:, lower].astype(F32)).astype(BF16)
        send(partial.at[1, :, lower], left_done.at[:, lower], c_s.at[0, c], c_r.at[0, c], to_right)
        received(from_right.at[:, lower], o_s.at[1, c], o_r.at[1, c])
        partial[2, :, higher] = (partial[2, :, higher].astype(F32) + from_right[:, lower].astype(F32)).astype(BF16)
        send(partial.at[2, :, higher], right_done.at[:, higher], c_s.at[1, c], c_r.at[1, c], to_left)
    attend(x, 0)
    for c in range(2 * PIECES):
        output(0, 1, c * PIECE, PIECE)
    received(left_done.at[:, high], d_s.at[0], d_r.at[0])
    received(right_done.at[:, low], d_s.at[1], d_r.at[1])
    for c in range(PIECES):
        received(left_done.at[:, pl.ds(c * PIECE, PIECE)], c_s.at[0, c], c_r.at[0, c])
        received(right_done.at[:, pl.ds(HALF + c * PIECE, PIECE)], c_s.at[1, c], c_r.at[1, c])

    @pl.loop(0, BLOCK // ROWS)
    def _(i):
        at = pl.ds(pl.multiple_of(i * ROWS, ROWS), ROWS)
        projected = partial[0, at, :].astype(F32) + left_done[at, :].astype(F32) + right_done[at, :].astype(F32)
        out[at, :] = (x_raw[x, at, :].astype(F32) + mod_rows[4:5, :] * projected).astype(BF16)

    for copy in sent:
        copy.wait_send()


def shards(
    latent, context, cond, ctx_cond, w_shift, w_scale, w_gate, w_query, key_weight, value_weight, w_out, sink
):
    inverse = (THETA ** (-np.arange(HEAD // 4, dtype=np.float32) * np.float32(2.0) / np.float32(HEAD // 2))).astype(
        np.float32
    )
    inverse = jnp.asarray(np.tile(np.tile(inverse, 4)[None], (8, 1)))
    anywhere = pl.BlockSpec(memory_space=pl.ANY)
    inside = pl.BlockSpec(memory_space=pltpu.VMEM)
    dma = pltpu.SemaphoreType.DMA
    return pl.pallas_call(
        kernel,
        out_shape=pltpu.VMEM((BLOCK, WIDTH), BF16),
        in_specs=[anywhere] * 13,
        out_specs=inside,
        scratch_shapes=[
            pltpu.VMEM((NSP, 128), F32),
            pltpu.VMEM((NSP, 128), F32),
            pltpu.SMEM((16,), F32),
            pltpu.VMEM((8, 128), F32),
            pltpu.VMEM((NX, BLOCK, HEAD), F32),
            pltpu.VMEM((NX, BLOCK, HEAD), F32),
            pltpu.VMEM((NX, BLOCK, WIDTH), BF16),
            pltpu.VMEM((NX, BLOCK, 128), F32),
            pltpu.VMEM((NX, BLOCK, 128), F32),
            pltpu.VMEM((NX * BLOCK, WIDTH), BF16),
            pltpu.VMEM((2, WIDTH, 512), BF16),
            pltpu.VMEM((2, 256, WIDTH), BF16),
            pltpu.VMEM((3, 128, 512), BF16),
            pltpu.VMEM((CTX_ROWS, WIDTH), BF16),
            pltpu.VMEM((CTX_ROWS, WIDTH), BF16),
            pltpu.VMEM((NY, 24, 128), F32),
            pltpu.VMEM((NZ, 24, 128), F32),
            pltpu.VMEM((NT, 24, 128), F32),
            pltpu.VMEM((8, WIDTH), F32),
            pltpu.VMEM((2, 2, NX * BLOCK, 256), BF16),
            pltpu.VMEM((NX, 4, BLOCK, HEAD), BF16),
            pltpu.VMEM((NX + 2, 2, BLOCK, 512), BF16),
            pltpu.VMEM((2, NY, NZ, CTX_ROWS, 256), BF16),
            pltpu.VMEM((NX * BLOCK, 512), BF16),
            pltpu.VMEM((NX, BLOCK, WIDTH), BF16),
            pltpu.VMEM((BLOCK, HALF), BF16),
            pltpu.VMEM((BLOCK, HALF), BF16),
            pltpu.VMEM((BLOCK, WIDTH), BF16),
            pltpu.VMEM((BLOCK, WIDTH), BF16),
            dma((13,)), dma((12,)), dma((12,)), dma((4,)), dma((4,)),
            dma((3,)), dma((3,)), dma((7,)), dma((7,)), dma((7,)), dma((7,)),
            dma((7,)), dma((7,)), dma((8, 3)), dma((8, 3)), dma((8, 4)), dma((8, 4)),
            dma((4,)), dma((4,)), dma((4,)), dma((4,)),
            dma((2, PIECES)), dma((2, PIECES)), dma((2,)), dma((2,)), dma((2, PIECES)), dma((2, PIECES)),
        ],
        compiler_params=pltpu.CompilerParams(
            collective_id=0, has_side_effects=True, vmem_limit_bytes=60 * 1024 * 1024
        ),
    )(
        latent, context, cond.reshape(NSP, 128), ctx_cond.reshape(NSP, 128), w_shift, w_scale, w_gate,
        w_query, key_weight, value_weight, w_out, sink, inverse,
    )


def solution(mesh):
    in_specs = (
        P(("sp", "tp"), None), P("sp", None), P(), P(), P("sp", "tp"), P("sp", "tp"), P("sp", "tp"),
        P(None, "tp"), P(None, "tp"), P(None, "tp"), P("tp", None), P(),
    )
    out_specs = P(("sp", "tp"), None)
    return jax.shard_map(shards, mesh=mesh, in_specs=in_specs, out_specs=out_specs, check_vma=False)
```

time: 75.8 us -> 62.3 us (0.82)
  Pallas kernels: 73.7 us -> 61.4 us
  local copies, waits for them, and re-layouts: 1.87 us -> 0.8 us
    pallas_call x1, Pallas kernels: 73.7 us -> 61.4 us  [shards(): pl.pallas_call(kernel, out_shape=pltpu.VMEM((BLOCK, WIDTH), BF16), in_spe...]
    unnamed x1, local copies, waits for them, and re-layouts: 1.87 us -> 0.8 us
where the time goes in v2:
time: 62.3 us; the launch traced here: 62.2 us
  Pallas kernels  61.4 us (99%)
  local copies, waits for them, and re-layouts  0.8 us (1%)
    pallas_call x1, Pallas kernels, shards(): pl.pallas_call(kernel, out_shape=pltpu.VMEM((BLOCK, WIDTH), BF16), in_spe...  61.4 us

profile of v2, /device:TPU:1, one launch (start us, length us, event | category | flops | bytes accessed | tf_op | source)
XLA Modules:
  0.0 62.2 jit_solution(13174573452376033800)
XLA Ops:
  0.0 61.4 %shard_map.127 = bf16[64,4096]{1,0:T(8,128)(2,1)S(1)} custom-call(bf16[64,4096]{1,0:T(8,128)(2,1)} %latent.1, bf16[32,4096]{1,0:T(8,128)(2,1)} %context.1, f32[32,128]{1,0:T(8,128)} %bitcast.2, f32[32,128]{1,0:T(8,128)} %bitcast.3, bf16[128,512]{1,0:T(8,128)(2,1)} %w_shift.1, bf16[128,512]{1,0:T(8,128)(2,1)} %w_scale.1, bf16[128,512]{1,0:T(8,128)(2,1)} %w_gate.1, ...), custom_call_target="tpu_custom_call" | custom-call | tf_op jit(solution)/shard_map/pallas_call | solution.py:462
  61.4 0.8 %copy.15 = bf16[64,4096]{1,0:T(8,128)(2,1)} copy(bf16[64,4096]{1,0:T(8,128)(2,1)S(1)} %shard_map.127) | data formatting | bytes 1048576

commit v3 on v2

v3 whole, which is shorter than its diff:
```python
import jax
import jax.numpy as jnp
import numpy as np
from jax import lax
from jax.experimental import pallas as pl
from jax.experimental.pallas import tpu as pltpu
from jax.sharding import PartitionSpec as P

MESH = pl.DeviceIdType.MESH
F32 = jnp.float32
BF16 = jnp.bfloat16

NX, NY, NZ, NT = 4, 4, 8, 8
NSP = NY * NZ
HEAD = 128
SIDE = 128
BLOCK = 64
WIDTH = 4096
HALF = WIDTH // 2
PAIR = 2 * BLOCK
TOKENS = 16384
CTX_ROWS = 32
EPS = 1e-05
THETA = 10000.0
MASKED = -1e30
PIECES = 4
PIECE = HALF // PIECES
ROWS = 16
SINGLE = 34


def kernel(
    latent, context, cond_in, ctx_cond_in, w_shift, w_scale, w_gate, wq, wk, wv, wo, sink_in, inverse_in, out,
    cond, ctx_cond, sink, inverse, cosines, sines, x_raw, means, scales, x_mod, w_all, w_out, w_modulation, ctx_raw, ctx_mod, y_buf, z_buf, t_buf, zg_buf, tg_buf, mod_rows,
    product, query, kv, ckv, attended, partial, from_left, from_right, left_done, right_done,
    l_sem, ag_r, cz_r, cy_r, h_r, o_r, sems,
):
    sp = lax.axis_index("sp")
    tp = lax.axis_index("tp")
    z, y = sp // NY, sp % NY
    x, core = tp // 2, tp % 2
    sibling = x * 2 + 1 - core
    right, opposite, left = (x + 1) % NX, (x + 2) % NX, (x + 3) % NX
    sp_next, sp_back = (sp + 1) % NSP, (sp + NSP - 1) % NSP
    to_right, to_left = (sp, right * 2 + core), (sp, left * 2 + core)
    to_sibling = (sp, sibling)

    def remote(src, dst, send, recv, device):
        return pltpu.make_async_remote_copy(
            src_ref=src, dst_ref=dst, send_sem=send, recv_sem=recv, device_id=device, device_id_type=MESH
        )

    names = iter(range(SINGLE))

    def pair():
        return sems.at[next(names)], sems.at[next(names)]

    def send(*args):
        remote(*args).start()

    def received(ref, sem):
        remote(ref, ref, sem, sem, to_sibling).wait_recv()

    drains = []

    def drained_at_end(ref, sem):
        drains.append(remote(ref, ref, sem, sem, to_sibling))

    local = [
        pltpu.make_async_copy(cond_in, cond, l_sem.at[0]),
        pltpu.make_async_copy(ctx_cond_in, ctx_cond, l_sem.at[1]),
        pltpu.make_async_copy(w_shift, w_modulation.at[0], l_sem.at[2]),
        pltpu.make_async_copy(w_scale, w_modulation.at[1], l_sem.at[3]),
        pltpu.make_async_copy(w_gate, w_modulation.at[2], l_sem.at[4]),
        pltpu.make_async_copy(latent, x_raw.at[x], l_sem.at[5]),
        pltpu.make_async_copy(context, ctx_raw, l_sem.at[6]),
        pltpu.make_async_copy(sink_in, sink, l_sem.at[7]),
        pltpu.make_async_copy(inverse_in, inverse, l_sem.at[8]),
        pltpu.make_async_copy(wq, w_all.at[core, :, 0:256], l_sem.at[9]),
        pltpu.make_async_copy(wk, w_all.at[core, :, 256:384], l_sem.at[10]),
        pltpu.make_async_copy(wv, w_all.at[core, :, 384:512], l_sem.at[11]),
        pltpu.make_async_copy(wo, w_out.at[core], l_sem.at[12]),
    ]
    for copy in local[:6]:
        copy.start()

    barrier = pltpu.get_barrier_semaphore()
    greeted = [(sp, (tp + d) % NT) for d in range(1, NT)]
    greeted += [(z * NY + (y + d) % NY, tp) for d in range(1, NY)]
    greeted += [(((z + d) % NZ) * NY + y, tp) for d in range(1, NZ)]
    greeted += [(sp_next, tp), (sp_next, sibling), (sp_back, tp), (sp_back, sibling)]
    for device in greeted:
        pl.semaphore_signal(barrier, inc=1, device_id=device, device_id_type=MESH)

    local[0].wait()
    local[1].wait()
    act = jnp.concatenate(
        [jax.nn.silu(cond[pl.ds(sp, 1), :]), jax.nn.silu(ctx_cond[pl.ds(sp, 1), :]), jnp.zeros((6, 128), F32)],
        axis=0,
    ).astype(BF16)
    y_buf[y] = jnp.zeros((24, 128), F32)
    for i in range(3):
        local[2 + i].wait()
        part = jnp.dot(act, w_modulation[i], preferred_element_type=F32)
        for row in range(2 if i < 2 else 1):
            for c in range(4):
                at = (2 * i + row) * 4 + c
                y_buf[y, at : at + 1, :] = part[row : row + 1, c * 128 : (c + 1) * 128]

    pl.semaphore_wait(barrier, len(greeted))

    y_s, y_r = pair()
    for d in range(1, NY):
        send(y_buf.at[y], y_buf.at[y], y_s, y_r, (z * NY + (y + d) % NY, tp))
    drained_at_end(y_buf.at[0:3], y_s)

    local[5].wait()
    ag_s, _ = pair()
    drained_at_end(x_raw.at[0:3], ag_s)

    def rows_of(piece):
        return pl.ds(piece * ROWS, ROWS)

    def gather(block, piece, i, device):
        ref = x_raw.at[block, rows_of(piece), :]
        send(ref, ref, ag_s, ag_r.at[i], device)

    def own_pieces(i):
        gather(x, i, i, to_right)
        gather(x, 3 - i, 6 + i, to_left)

    def gathered(i):
        near = i < 4
        if near:
            received(x_raw.at[left, rows_of(i), :], ag_r.at[i])
            received(x_raw.at[right, rows_of(3 - i), :], ag_r.at[6 + i])
        else:
            received(x_raw.at[opposite, rows_of(i - 4), :], ag_r.at[i])
            received(x_raw.at[opposite, rows_of(7 - i), :], ag_r.at[6 + i])

    def forward(i):
        gather(left, i, 4 + i, to_right)
        gather(right, 3 - i, 10 + i, to_left)

    own_pieces(0)
    own_pieces(1)

    for copy in local[6:]:
        copy.start()

    w_s, w_r = pair()
    send(wq, w_all.at[core, :, 0:256], w_s, w_r, to_sibling)
    send(wk, w_all.at[core, :, 256:384], w_s, w_r, to_sibling)
    send(wv, w_all.at[core, :, 384:512], w_s, w_r, to_sibling)
    drained_at_end(w_all.at[core], w_s)

    def moments(read, rows):
        chunks = [slice(i * 128, (i + 1) * 128) for i in range(WIDTH // 128)]
        mean = jnp.sum(sum(read(at).astype(F32) for at in chunks), axis=-1, keepdims=True) / WIDTH
        mean = jnp.broadcast_to(mean, (rows, 128))
        var = sum(jnp.square(read(at).astype(F32) - mean) for at in chunks)
        var = jnp.sum(var, axis=-1, keepdims=True) / WIDTH
        return mean, jnp.broadcast_to(lax.rsqrt(var + EPS), (rows, 128))

    def statistics(block, half):
        rows = slice(half * 32, half * 32 + 32)
        means[block, rows, :], scales[block, rows, :] = moments(lambda at: x_raw[block, rows, at], 32)

    @pl.loop(0, 2)
    def _(i):
        at = pl.ds(pl.multiple_of(i * 32, 32), 32)
        means[x, at, :], scales[x, at, :] = moments(lambda columns: x_raw[x, at, columns], 32)

    lane = lax.broadcasted_iota(jnp.int32, (BLOCK, HEAD), 1)
    column = lax.broadcasted_iota(jnp.int32, (BLOCK, HEAD), 0)
    by_row = lane < HEAD // 2
    is_first = lane % (HEAD // 2) < HEAD // 4

    local[7].wait()
    local[8].wait()

    @pl.loop(0, NX)
    def _(b):
        position = jnp.where(by_row, sp * NT + b * 2 + core, column).astype(F32)
        angle = position * inverse[0:1, :]
        cosines[b] = jnp.cos(angle)
        sine = jnp.sin(angle)
        sines[b] = jnp.where(is_first, -sine, sine)

    received(y_buf.at[0:3], y_r)
    total = jnp.sum(y_buf[...], axis=0)
    z_buf[z] = total[0:16]
    zg_buf[z] = total[16:24]
    z_s, z_r = pair()
    for d in (4, 3, 5, 2, 6, 1, 7):
        send(z_buf.at[z], z_buf.at[z], z_s, z_r, (((z + d) % NZ) * NY + y, tp))
    drained_at_end(z_buf.at[0:7], z_s)
    own_pieces(2)
    received(z_buf.at[0:7], z_r)
    t_buf[tp] = jnp.sum(z_buf[...], axis=0)
    t_s, t_r = pair()
    for d in (4, 5, 3, 2, 6, 7, 1):
        send(t_buf.at[tp], t_buf.at[tp], t_s, t_r, (sp, (tp + d) % NT))
    drained_at_end(t_buf.at[0:7], t_s)
    own_pieces(3)
    zg_s, zg_r = pair()
    for d in range(1, NZ):
        send(zg_buf.at[z], zg_buf.at[z], zg_s, zg_r, (((z + d) % NZ) * NY + y, tp))
    drained_at_end(zg_buf.at[0:7], zg_s)
    wo_s, wo_r = pair()
    send(wo, w_out.at[core], wo_s, wo_r, to_sibling)
    drained_at_end(w_out.at[core], wo_s)

    for i in range(2):
        gathered(i)
        forward(i)

    statistics(left, 0)
    statistics(right, 1)
    local[6].wait()
    ctx_mean, ctx_scale = moments(lambda at: ctx_raw[:, at], CTX_ROWS)

    received(t_buf.at[0:7], t_r)
    for t in range(NT):
        values = t_buf[t]
        for row in range(4):
            for c in range(4):
                at = t * 512 + c * 128
                value = values[row * 4 + c : row * 4 + c + 1, :]
                mod_rows[row : row + 1, at : at + 128] = 1.0 + value if row > 1 else value

    for i in range(WIDTH // 128):
        at = slice(i * 128, (i + 1) * 128)
        normal = (ctx_raw[:, at].astype(F32) - ctx_mean) * ctx_scale
        ctx_mod[:, at] = (normal * mod_rows[3:4, at] + mod_rows[1:2, at]).astype(BF16)
    for copy in local[9:]:
        copy.wait()
    halves = [
        jnp.dot(ctx_mod[:, at], w_all[core, at, 256:512], preferred_element_type=F32)
        for at in (slice(0, HALF), slice(HALF, WIDTH))
    ]
    ckv[core, y, z] = (halves[0] + halves[1]).astype(BF16)

    cz_s, _ = pair()
    cy_s, cw_s = pair()
    cc_s, cc_r = pair()

    near_z = (1, 7, 2, 6)

    def spread(d):
        line = ckv.at[core, y, (z + NZ - d) % NZ]
        if d:
            received(line, cz_r.at[d - 1])
        if d not in near_z:
            for e in (2, 1, 3):
                send(line, line, cy_s, cy_r.at[d], (z * NY + (y + e) % NY, tp))
        send(line, line, cc_s, cc_r, to_sibling)

    def relay(d):
        there = (z + NZ - d) % NZ
        received(ckv.at[core, 0:3, there], cy_r.at[d])
        for e in range(1, NY):
            line = ckv.at[core, (y + NY - e) % NY, there]
            if d == 0:
                for f in near_z:
                    send(line, line, cw_s, cy_r.at[f], (((z + f) % NZ) * NY + y, tp))
            send(line, line, cc_s, cc_r, to_sibling)

    own = ckv.at[core, y, z]
    for d in (4, 3, 5, 2, 6, 1, 7):
        send(own, own, cz_s, cz_r.at[d - 1], (((z + d) % NZ) * NY + y, tp))
    drained_at_end(ckv.at[core, 0, 0:7], cz_s)
    drained_at_end(ckv.at[0, 0:3, 0:4], cy_s)
    drained_at_end(ckv.at[0, 0:3, 0:4], cw_s)
    drained_at_end(ckv.at[core], cc_s)
    spread(0)

    blocks = (x, right, left, opposite)

    def modulate(slot):
        block = blocks[slot]

        @pl.loop(0, WIDTH // 512)
        def _(c):
            for q in range(4):
                at = pl.ds(pl.multiple_of(c * 512 + q * 128, 128), 128)
                normal = (x_raw[block, :, at].astype(F32) - means[block]) * scales[block]
                x_mod[slot * BLOCK : (slot + 1) * BLOCK, at] = (
                    normal * mod_rows[2:3, at] + mod_rows[0:1, at]
                ).astype(BF16)

    modulate(0)
    gathered(2)
    gathered(3)

    statistics(left, 1)
    statistics(right, 0)

    modulate(1)
    modulate(2)

    def project(c, slot, slots):
        rows = slice(slot * BLOCK, (slot + slots) * BLOCK)
        for j in range(2):
            product[j, c, rows, :] = jnp.dot(
                x_mod[rows, :], w_all[j, :, c * 256 : (c + 1) * 256], preferred_element_type=F32
            ).astype(BF16)

    def place(slot):
        return (x + slot + slot // 2 * (5 - 2 * slot)) % NX, pl.ds(pl.multiple_of(slot * BLOCK, BLOCK), BLOCK)

    def turned(value, b):
        value = value.astype(F32)
        partner = jnp.where(is_first, pltpu.roll(value, 96, 1), pltpu.roll(value, 32, 1))
        return (value * cosines[b] + partner * sines[b]).astype(BF16)

    def turn_keys(slot):
        b, rows = place(slot)
        for j in range(2):
            kv[b + 1, core, j] = turned(product[j, 1, rows, 0:HEAD], b)
            kv[b + 1, core, 2 + j] = product[j, 1, rows, HEAD : 2 * HEAD]

    def turn_queries(slot):
        b, rows = place(slot)
        for j in range(2):
            for g in range(2):
                query[b, 2 * j + g] = turned(product[j, 0, rows, g * HEAD : (g + 1) * HEAD], b)

    kv_s, kv_r = pair()
    drained_at_end(kv.at[1:5, core], kv_s)

    def share(slot):
        ref = kv.at[blocks[slot] + 1, core]
        send(ref, ref, kv_s, kv_r, to_sibling)

    h_s, _ = pair()
    drained_at_end(kv.at[1:4, core], h_s)
    to_next = remote(kv.at[NX, core], kv.at[0, core], h_s, h_r.at[0], (sp_next, tp))
    to_back = remote(kv.at[1, core], kv.at[NX + 1, core], h_s, h_r.at[2], (sp_back, tp))
    to_next_other = remote(kv.at[NX, core], kv.at[0, core], h_s, h_r.at[1], (sp_next, sibling))
    to_back_other = remote(kv.at[1, core], kv.at[NX + 1, core], h_s, h_r.at[3], (sp_back, sibling))
    kv[(NX + 1) * (1 - core), 1 - core] = jnp.zeros((4, BLOCK, HEAD), BF16)

    def halo_when(last, first):
        @pl.when(last)
        def _():
            to_next.start()

            @pl.when(core == 1)
            def _():
                to_next_other.start()

        @pl.when(first)
        def _():
            to_back.start()

            @pl.when(core == 0)
            def _():
                to_back_other.start()

    def halo_received(first, last):
        @pl.when(first)
        def _():
            received(kv.at[0, core], h_r.at[0])

            @pl.when(core == 0)
            def _():
                received(kv.at[0, 1], h_r.at[1])

        @pl.when(last)
        def _():
            received(kv.at[NX + 1, core], h_r.at[2])

            @pl.when(core == 1)
            def _():
                received(kv.at[NX + 1, 0], h_r.at[3])

    other = w_all.at[1 - core]
    received(other, w_r)
    project(1, 0, 3)
    relay(0)

    @pl.loop(0, 3)
    def _(slot):
        turn_keys(slot)

    for slot in range(3):
        share(slot)
    halo_when(opposite != NX - 1, opposite != 0)
    for d in (3, 5, 4, 1, 7, 2, 6):
        spread(d)
    project(0, 0, 3)

    @pl.loop(0, 3)
    def _(slot):
        turn_queries(slot)

    gathered(4)
    gathered(5)

    received(zg_buf.at[0:7], zg_r)
    tg_buf[tp] = jnp.sum(zg_buf[...], axis=0)
    tg_s, tg_r = pair()
    for d in range(1, NT):
        send(tg_buf.at[tp], tg_buf.at[tp], tg_s, tg_r, (sp, (tp + d) % NT))
    drained_at_end(tg_buf.at[0:7], tg_s)

    statistics(opposite, 0)
    statistics(opposite, 1)
    modulate(3)
    project(1, 3, 1)
    turn_keys(3)
    share(3)
    halo_when(opposite == NX - 1, opposite == 0)
    for d in (1, 7, 2, 6):
        relay(d)
    project(0, 3, 1)
    turn_queries(3)
    for d in (3, 5, 4):
        relay(d)
    received(kv.at[1:5, 1 - core], kv_r)
    halo_received(opposite == 0, opposite == NX - 1)

    factor = HEAD ** (-0.5)
    i_query = lax.broadcasted_iota(jnp.int32, (PAIR, 3 * PAIR), 0) % BLOCK + core * BLOCK
    i_key = lax.broadcasted_iota(jnp.int32, (PAIR, 3 * PAIR), 1) - PAIR
    near = jnp.abs(i_key - i_query) <= SIDE
    upper = lax.broadcasted_iota(jnp.int32, (PAIR, 1), 0) < BLOCK
    across = (((1,), (1,)), ((), ()))

    def attend(b, slot, heads=(0, 1)):
        key_at = i_key + (sp * NT * BLOCK + b * PAIR)
        valid = near & (key_at >= 0) & (key_at < TOKENS)
        for h in heads:
            q = query[b, pl.ds(2 * h, 2)].reshape(PAIR, HEAD)
            k_band = kv[pl.ds(b, 3), :, h].reshape(3 * PAIR, HEAD)
            v_band = kv[pl.ds(b, 3), :, 2 + h].reshape(3 * PAIR, HEAD)
            k_ctx = ckv[h, :, :, :, 0:HEAD].reshape(NSP * CTX_ROWS, HEAD)
            v_ctx = ckv[h, :, :, :, HEAD : 2 * HEAD].reshape(NSP * CTX_ROWS, HEAD)
            s_band = lax.dot_general(q, k_band, across, preferred_element_type=F32) * factor
            s_band = jnp.where(valid, s_band, MASKED)
            s_ctx = lax.dot_general(q, k_ctx, across, preferred_element_type=F32) * factor
            sinks = jnp.where(upper, sink[4 * x + 2 * h], sink[4 * x + 2 * h + 1])
            top = jnp.maximum(
                jnp.maximum(jnp.max(s_band, axis=-1, keepdims=True), jnp.max(s_ctx, axis=-1, keepdims=True)), sinks
            )
            e_band = jnp.exp(s_band - top)
            e_ctx = jnp.exp(s_ctx - top)
            total = (
                jnp.sum(e_band, axis=-1, keepdims=True)
                + jnp.sum(e_ctx, axis=-1, keepdims=True)
                + jnp.exp(sinks - top)
            )
            value = jnp.dot(e_band.astype(BF16), v_band, preferred_element_type=F32)
            value += jnp.dot(e_ctx.astype(BF16), v_ctx, preferred_element_type=F32)
            value = (value / total).astype(BF16)
            rows = slice(slot * BLOCK, (slot + 1) * BLOCK)
            for g in range(2):
                attended[h, rows, g * HEAD : (g + 1) * HEAD] = value[g * BLOCK : (g + 1) * BLOCK]

    def output(slot, slots, at, width):
        rows = slice(slot * BLOCK, (slot + slots) * BLOCK)
        columns = slice(at, at + width)
        result = jnp.dot(attended[0, rows, :], w_out[0, :, columns], preferred_element_type=F32)
        result += jnp.dot(attended[1, rows, :], w_out[1, :, columns], preferred_element_type=F32)
        result = result.astype(BF16)
        for s in range(slots):
            partial[slot + s, :, columns] = result[s * BLOCK : (s + 1) * BLOCK]

    attend(opposite, 3, (core,))
    received(ckv.at[1 - core], cc_r)
    attend(opposite, 3, (1 - core,))
    received(w_out.at[1 - core], wo_r)
    o_s, d_s = pair()
    c_s, _ = pair()
    left_r, right_r = pair()
    for sem in (o_s, d_s, c_s):
        drained_at_end(partial.at[0], sem)
    for c in range(PIECES):
        output(3, 1, c * PIECE, PIECE)
        output(3, 1, HALF + c * PIECE, PIECE)
        lower = pl.ds(c * PIECE, PIECE)
        higher = pl.ds(HALF + c * PIECE, PIECE)
        send(partial.at[3, :, lower], from_left.at[:, lower], o_s, o_r.at[0, c], to_right)
        send(partial.at[3, :, higher], from_right.at[:, lower], o_s, o_r.at[1, c], to_left)
    halo_received(opposite != 0, opposite != NX - 1)
    attend(right, 1)
    attend(left, 2)
    for c in range(2 * PIECES):
        output(1, 2, c * PIECE, PIECE)
    low, high = pl.ds(0, HALF), pl.ds(HALF, HALF)
    send(partial.at[1, :, high], left_done.at[:, high], d_s, left_r, to_right)
    send(partial.at[2, :, low], right_done.at[:, low], d_s, right_r, to_left)
    for c in range(PIECES):
        lower = pl.ds(c * PIECE, PIECE)
        higher = pl.ds(HALF + c * PIECE, PIECE)
        received(from_left.at[:, lower], o_r.at[0, c])
        partial[1, :, lower] = (partial[1, :, lower].astype(F32) + from_left[:, lower].astype(F32)).astype(BF16)
        send(partial.at[1, :, lower], left_done.at[:, lower], c_s, left_r, to_right)
        received(from_right.at[:, lower], o_r.at[1, c])
        partial[2, :, higher] = (partial[2, :, higher].astype(F32) + from_right[:, lower].astype(F32)).astype(BF16)
        send(partial.at[2, :, higher], right_done.at[:, higher], c_s, right_r, to_left)
    attend(x, 0)
    for c in range(2 * PIECES):
        output(0, 1, c * PIECE, PIECE)
    received(tg_buf.at[0:7], tg_r)
    for t in range(NT):
        for c in range(4):
            at = t * 512 + c * 128
            mod_rows[4:5, at : at + 128] = tg_buf[t, c : c + 1, :]
    received(left_done, left_r)
    received(right_done, right_r)

    @pl.loop(0, BLOCK // ROWS)
    def _(i):
        at = pl.ds(pl.multiple_of(i * ROWS, ROWS), ROWS)
        projected = partial[0, at, :].astype(F32) + left_done[at, :].astype(F32) + right_done[at, :].astype(F32)
        out[at, :] = (x_raw[x, at, :].astype(F32) + mod_rows[4:5, :] * projected).astype(BF16)

    for copy in drains:
        copy.wait_send()


def shards(
    latent, context, cond, ctx_cond, w_shift, w_scale, w_gate, w_query, key_weight, value_weight, w_out, sink
):
    inverse = (THETA ** (-np.arange(HEAD // 4, dtype=np.float32) * np.float32(2.0) / np.float32(HEAD // 2))).astype(
        np.float32
    )
    inverse = jnp.asarray(np.tile(np.tile(inverse, 4)[None], (8, 1)))
    anywhere = pl.BlockSpec(memory_space=pl.ANY)
    inside = pl.BlockSpec(memory_space=pltpu.VMEM)
    dma = pltpu.SemaphoreType.DMA
    return pl.pallas_call(
        kernel,
        out_shape=pltpu.VMEM((BLOCK, WIDTH), BF16),
        in_specs=[anywhere] * 13,
        out_specs=inside,
        scratch_shapes=[
            pltpu.VMEM((NSP, 128), F32),
            pltpu.VMEM((NSP, 128), F32),
            pltpu.SMEM((16,), F32),
            pltpu.VMEM((8, 128), F32),
            pltpu.VMEM((NX, BLOCK, HEAD), F32),
            pltpu.VMEM((NX, BLOCK, HEAD), F32),
            pltpu.VMEM((NX, BLOCK, WIDTH), BF16),
            pltpu.VMEM((NX, BLOCK, 128), F32),
            pltpu.VMEM((NX, BLOCK, 128), F32),
            pltpu.VMEM((NX * BLOCK, WIDTH), BF16),
            pltpu.VMEM((2, WIDTH, 512), BF16),
            pltpu.VMEM((2, 256, WIDTH), BF16),
            pltpu.VMEM((3, 128, 512), BF16),
            pltpu.VMEM((CTX_ROWS, WIDTH), BF16),
            pltpu.VMEM((CTX_ROWS, WIDTH), BF16),
            pltpu.VMEM((NY, 24, 128), F32),
            pltpu.VMEM((NZ, 16, 128), F32),
            pltpu.VMEM((NT, 16, 128), F32),
            pltpu.VMEM((NZ, 8, 128), F32),
            pltpu.VMEM((NT, 8, 128), F32),
            pltpu.VMEM((8, WIDTH), F32),
            pltpu.VMEM((2, 2, NX * BLOCK, 256), BF16),
            pltpu.VMEM((NX, 4, BLOCK, HEAD), BF16),
            pltpu.VMEM((NX + 2, 2, 4, BLOCK, HEAD), BF16),
            pltpu.VMEM((2, NY, NZ, CTX_ROWS, 256), BF16),
            pltpu.VMEM((2, NX * BLOCK, 2 * HEAD), BF16),
            pltpu.VMEM((NX, BLOCK, WIDTH), BF16),
            pltpu.VMEM((BLOCK, HALF), BF16),
            pltpu.VMEM((BLOCK, HALF), BF16),
            pltpu.VMEM((BLOCK, WIDTH), BF16),
            pltpu.VMEM((BLOCK, WIDTH), BF16),
            dma((13,)), dma((12,)), dma((7,)), dma((8,)), dma((4,)), dma((2, PIECES)), dma((SINGLE,)),
        ],
        compiler_params=pltpu.CompilerParams(
            collective_id=0, has_side_effects=True, vmem_limit_bytes=60 * 1024 * 1024
        ),
    )(
        latent, context, cond.reshape(NSP, 128), ctx_cond.reshape(NSP, 128), w_shift, w_scale, w_gate,
        w_query, key_weight, value_weight, w_out, sink, inverse,
    )


def solution(mesh):
    in_specs = (
        P(("sp", "tp"), None), P("sp", None), P(), P(), P("sp", "tp"), P("sp", "tp"), P("sp", "tp"),
        P(None, "tp"), P(None, "tp"), P(None, "tp"), P("tp", None), P(),
    )
    out_specs = P(("sp", "tp"), None)
    return jax.shard_map(shards, mesh=mesh, in_specs=in_specs, out_specs=out_specs, check_vma=False)
```

time: 62.3 us -> 57.1 us (0.917)
  Pallas kernels: 61.4 us -> 56.1 us
    pallas_call x1, Pallas kernels: 61.4 us -> 56.1 us  [shards(): pl.pallas_call(kernel, out_shape=pltpu.VMEM((BLOCK, WIDTH), BF16), in_spe...]
where the time goes in v3:
time: 57.1 us; the launch traced here: 56.9 us
  Pallas kernels  56.1 us (98%)
  local copies, waits for them, and re-layouts  0.8 us (1%)
    pallas_call x1, Pallas kernels, shards(): pl.pallas_call(kernel, out_shape=pltpu.VMEM((BLOCK, WIDTH), BF16), in_spe...  56.1 us

profile of v3, /device:TPU:1, one launch (start us, length us, event | category | flops | bytes accessed | tf_op | source)
XLA Modules:
  0.0 56.9 jit_solution(11211822378648019567)
XLA Ops:
  0.0 56.1 %shard_map.127 = bf16[64,4096]{1,0:T(8,128)(2,1)S(1)} custom-call(bf16[64,4096]{1,0:T(8,128)(2,1)} %latent.1, bf16[32,4096]{1,0:T(8,128)(2,1)} %context.1, f32[32,128]{1,0:T(8,128)} %bitcast.2, f32[32,128]{1,0:T(8,128)} %bitcast.3, bf16[128,512]{1,0:T(8,128)(2,1)} %w_shift.1, bf16[128,512]{1,0:T(8,128)(2,1)} %w_scale.1, bf16[128,512]{1,0:T(8,128)(2,1)} %w_gate.1, ...), custom_call_target="tpu_custom_call" | custom-call | tf_op jit(solution)/shard_map/pallas_call | solution.py:534
  56.2 0.8 %copy.15 = bf16[64,4096]{1,0:T(8,128)(2,1)} copy(bf16[64,4096]{1,0:T(8,128)(2,1)S(1)} %shard_map.127) | data formatting | bytes 1048576

commit v4 on v3

--- a/solution.py
+++ b/solution.py
@@ -26,14 +26,14 @@
 PIECES = 4
 PIECE = HALF // PIECES
 ROWS = 16
-SINGLE = 34
+SINGLE = 27
 
 
 def kernel(
     latent, context, cond_in, ctx_cond_in, w_shift, w_scale, w_gate, wq, wk, wv, wo, sink_in, inverse_in, out,
-    cond, ctx_cond, sink, inverse, cosines, sines, x_raw, means, scales, x_mod, w_all, w_out, w_modulation, ctx_raw, ctx_mod, y_buf, z_buf, t_buf, zg_buf, tg_buf, mod_rows,
+    conds, sink, inverse, cosines, sines, x_raw, means, scales, x_mod, w_all, w_out, w_modulation, ctx_raw, ctx_mod, y_buf, z_buf, t_buf, zg_buf, tg_buf, mod_rows,
     product, query, kv, ckv, attended, partial, from_left, from_right, left_done, right_done,
-    l_sem, ag_r, cz_r, cy_r, h_r, o_r, sems,
+    l_sem, ag_r, cy_r, h_r, o_r, c_r, sems,
 ):
     sp = lax.axis_index("sp")
     tp = lax.axis_index("tp")
@@ -52,8 +52,11 @@
 
     names = iter(range(SINGLE))
 
+    def one():
+        return sems.at[next(names)]
+
     def pair():
-        return sems.at[next(names)], sems.at[next(names)]
+        return one(), one()
 
     def send(*args):
         remote(*args).start()
@@ -67,22 +70,25 @@
         drains.append(remote(ref, ref, sem, sem, to_sibling))
 
     local = [
-        pltpu.make_async_copy(cond_in, cond, l_sem.at[0]),
-        pltpu.make_async_copy(ctx_cond_in, ctx_cond, l_sem.at[1]),
-        pltpu.make_async_copy(w_shift, w_modulation.at[0], l_sem.at[2]),
-        pltpu.make_async_copy(w_scale, w_modulation.at[1], l_sem.at[3]),
-        pltpu.make_async_copy(w_gate, w_modulation.at[2], l_sem.at[4]),
-        pltpu.make_async_copy(latent, x_raw.at[x], l_sem.at[5]),
-        pltpu.make_async_copy(context, ctx_raw, l_sem.at[6]),
-        pltpu.make_async_copy(sink_in, sink, l_sem.at[7]),
-        pltpu.make_async_copy(inverse_in, inverse, l_sem.at[8]),
-        pltpu.make_async_copy(wq, w_all.at[core, :, 0:256], l_sem.at[9]),
-        pltpu.make_async_copy(wk, w_all.at[core, :, 256:384], l_sem.at[10]),
-        pltpu.make_async_copy(wv, w_all.at[core, :, 384:512], l_sem.at[11]),
-        pltpu.make_async_copy(wo, w_out.at[core], l_sem.at[12]),
+        pltpu.make_async_copy(cond_in, conds.at[0], l_sem.at[0]),
+        pltpu.make_async_copy(ctx_cond_in, conds.at[1], l_sem.at[0]),
+        pltpu.make_async_copy(w_shift, w_modulation.at[0], l_sem.at[1]),
+        pltpu.make_async_copy(w_scale, w_modulation.at[1], l_sem.at[1]),
+        pltpu.make_async_copy(w_gate, w_modulation.at[2], l_sem.at[1]),
+        pltpu.make_async_copy(latent, x_raw.at[x], l_sem.at[2]),
+        pltpu.make_async_copy(context, ctx_raw, l_sem.at[3]),
+        pltpu.make_async_copy(sink_in, sink, l_sem.at[4]),
+        pltpu.make_async_copy(inverse_in, inverse, l_sem.at[5]),
+        pltpu.make_async_copy(wq, w_all.at[core, :, 0:256], l_sem.at[6]),
+        pltpu.make_async_copy(wk, w_all.at[core, :, 256:384], l_sem.at[6]),
+        pltpu.make_async_copy(wv, w_all.at[core, :, 384:512], l_sem.at[6]),
+        pltpu.make_async_copy(wo, w_out.at[core], l_sem.at[7]),
     ]
     for copy in local[:6]:
         copy.start()
+
+    def copied(ref, i):
+        pltpu.make_async_copy(ref, ref, l_sem.at[i]).wait()
 
     barrier = pltpu.get_barrier_semaphore()
     greeted = [(sp, (tp + d) % NT) for d in range(1, NT)]
@@ -92,15 +98,14 @@
     for device in greeted:
         pl.semaphore_signal(barrier, inc=1, device_id=device, device_id_type=MESH)
 
-    local[0].wait()
-    local[1].wait()
+    copied(conds, 0)
     act = jnp.concatenate(
-        [jax.nn.silu(cond[pl.ds(sp, 1), :]), jax.nn.silu(ctx_cond[pl.ds(sp, 1), :]), jnp.zeros((6, 128), F32)],
+        [jax.nn.silu(conds[0, pl.ds(sp, 1), :]), jax.nn.silu(conds[1, pl.ds(sp, 1), :]), jnp.zeros((6, 128), F32)],
         axis=0,
     ).astype(BF16)
     y_buf[y] = jnp.zeros((24, 128), F32)
+    copied(w_modulation, 1)
     for i in range(3):
-        local[2 + i].wait()
         part = jnp.dot(act, w_modulation[i], preferred_element_type=F32)
         for row in range(2 if i < 2 else 1):
             for c in range(4):
@@ -115,7 +120,7 @@
     drained_at_end(y_buf.at[0:3], y_s)
 
     local[5].wait()
-    ag_s, _ = pair()
+    ag_s = one()
     drained_at_end(x_raw.at[0:3], ag_s)
 
     def rows_of(piece):
@@ -126,21 +131,16 @@
         send(ref, ref, ag_s, ag_r.at[i], device)
 
     def own_pieces(i):
-        gather(x, i, i, to_right)
-        gather(x, 3 - i, 6 + i, to_left)
+        gather(x, i, min(i, 2), to_right)
+        gather(x, 3 - i, 3 + i if i < 2 else 2, to_left)
 
     def gathered(i):
-        near = i < 4
-        if near:
-            received(x_raw.at[left, rows_of(i), :], ag_r.at[i])
-            received(x_raw.at[right, rows_of(3 - i), :], ag_r.at[6 + i])
-        else:
-            received(x_raw.at[opposite, rows_of(i - 4), :], ag_r.at[i])
-            received(x_raw.at[opposite, rows_of(7 - i), :], ag_r.at[6 + i])
+        received(x_raw.at[left, rows_of(i), :], ag_r.at[i])
+        received(x_raw.at[right, rows_of(3 - i), :], ag_r.at[3 + i])
 
     def forward(i):
-        gather(left, i, 4 + i, to_right)
-        gather(right, 3 - i, 10 + i, to_left)
+        gather(left, i, 5, to_right)
+        gather(right, 3 - i, 5, to_left)
 
     own_pieces(0)
     own_pieces(1)
@@ -233,46 +233,40 @@
         at = slice(i * 128, (i + 1) * 128)
         normal = (ctx_raw[:, at].astype(F32) - ctx_mean) * ctx_scale
         ctx_mod[:, at] = (normal * mod_rows[3:4, at] + mod_rows[1:2, at]).astype(BF16)
-    for copy in local[9:]:
-        copy.wait()
+    copied(w_all.at[core], 6)
+    local[12].wait()
     halves = [
         jnp.dot(ctx_mod[:, at], w_all[core, at, 256:512], preferred_element_type=F32)
         for at in (slice(0, HALF), slice(HALF, WIDTH))
     ]
     ckv[core, y, z] = (halves[0] + halves[1]).astype(BF16)
 
-    cz_s, _ = pair()
-    cy_s, cw_s = pair()
-    cc_s, cc_r = pair()
+    cz_s, cz_r = pair()
+    ctx_s, cc_r = pair()
 
     near_z = (1, 7, 2, 6)
 
     def spread(d):
         line = ckv.at[core, y, (z + NZ - d) % NZ]
-        if d:
-            received(line, cz_r.at[d - 1])
         if d not in near_z:
             for e in (2, 1, 3):
-                send(line, line, cy_s, cy_r.at[d], (z * NY + (y + e) % NY, tp))
-        send(line, line, cc_s, cc_r, to_sibling)
+                send(line, line, ctx_s, cy_r.at[min(d, 1)], (z * NY + (y + e) % NY, tp))
+        send(line, line, ctx_s, cc_r, to_sibling)
 
     def relay(d):
         there = (z + NZ - d) % NZ
-        received(ckv.at[core, 0:3, there], cy_r.at[d])
         for e in range(1, NY):
             line = ckv.at[core, (y + NY - e) % NY, there]
             if d == 0:
                 for f in near_z:
-                    send(line, line, cw_s, cy_r.at[f], (((z + f) % NZ) * NY + y, tp))
-            send(line, line, cc_s, cc_r, to_sibling)
+                    send(line, line, ctx_s, cy_r.at[2], (((z + f) % NZ) * NY + y, tp))
+            send(line, line, ctx_s, cc_r, to_sibling)
 
     own = ckv.at[core, y, z]
     for d in (4, 3, 5, 2, 6, 1, 7):
-        send(own, own, cz_s, cz_r.at[d - 1], (((z + d) % NZ) * NY + y, tp))
+        send(own, own, cz_s, cz_r, (((z + d) % NZ) * NY + y, tp))
     drained_at_end(ckv.at[core, 0, 0:7], cz_s)
-    drained_at_end(ckv.at[0, 0:3, 0:4], cy_s)
-    drained_at_end(ckv.at[0, 0:3, 0:4], cw_s)
-    drained_at_end(ckv.at[core], cc_s)
+    drained_at_end(ckv.at[0:2, 0:4, 0:7], ctx_s)
     spread(0)
 
     blocks = (x, right, left, opposite)
@@ -290,8 +284,7 @@
                 ).astype(BF16)
 
     modulate(0)
-    gathered(2)
-    gathered(3)
+    received(x_raw.at[left], ag_r.at[2])
 
     statistics(left, 1)
     statistics(right, 0)
@@ -333,7 +326,7 @@
         ref = kv.at[blocks[slot] + 1, core]
         send(ref, ref, kv_s, kv_r, to_sibling)
 
-    h_s, _ = pair()
+    h_s = one()
     drained_at_end(kv.at[1:4, core], h_s)
     to_next = remote(kv.at[NX, core], kv.at[0, core], h_s, h_r.at[0], (sp_next, tp))
     to_back = remote(kv.at[1, core], kv.at[NX + 1, core], h_s, h_r.at[2], (sp_back, tp))
@@ -378,6 +371,7 @@
     other = w_all.at[1 - core]
     received(other, w_r)
     project(1, 0, 3)
+    received(ckv.at[core, 0:3, 0], cy_r.at[0])
     relay(0)
 
     @pl.loop(0, 3)
@@ -387,16 +381,16 @@
     for slot in range(3):
         share(slot)
     halo_when(opposite != NX - 1, opposite != 0)
+    project(0, 0, 3)
+
+    received(ckv.at[core, 0, 0:7], cz_r)
     for d in (3, 5, 4, 1, 7, 2, 6):
         spread(d)
-    project(0, 0, 3)
-
     @pl.loop(0, 3)
     def _(slot):
         turn_queries(slot)
 
-    gathered(4)
-    gathered(5)
+    received(x_raw.at[opposite], ag_r.at[5])
 
     received(zg_buf.at[0:7], zg_r)
     tg_buf[tp] = jnp.sum(zg_buf[...], axis=0)
@@ -412,16 +406,19 @@
     turn_keys(3)
     share(3)
     halo_when(opposite == NX - 1, opposite == 0)
+    project(0, 3, 1)
+    turn_queries(3)
+    received(ckv.at[core, 0:3, 0:4], cy_r.at[2])
     for d in (1, 7, 2, 6):
         relay(d)
-    project(0, 3, 1)
-    turn_queries(3)
+    received(ckv.at[core, 0:3, 0:3], cy_r.at[1])
     for d in (3, 5, 4):
         relay(d)
     received(kv.at[1:5, 1 - core], kv_r)
     halo_received(opposite == 0, opposite == NX - 1)
 
-    factor = HEAD ** (-0.5)
+    power = HEAD ** (-0.5) * np.log2(np.e).item()
+    to_scores = HEAD**0.5
     i_query = lax.broadcasted_iota(jnp.int32, (PAIR, 3 * PAIR), 0) % BLOCK + core * BLOCK
     i_key = lax.broadcasted_iota(jnp.int32, (PAIR, 3 * PAIR), 1) - PAIR
     near = jnp.abs(i_key - i_query) <= SIDE
@@ -437,19 +434,19 @@
             v_band = kv[pl.ds(b, 3), :, 2 + h].reshape(3 * PAIR, HEAD)
             k_ctx = ckv[h, :, :, :, 0:HEAD].reshape(NSP * CTX_ROWS, HEAD)
             v_ctx = ckv[h, :, :, :, HEAD : 2 * HEAD].reshape(NSP * CTX_ROWS, HEAD)
-            s_band = lax.dot_general(q, k_band, across, preferred_element_type=F32) * factor
+            s_band = lax.dot_general(q, k_band, across, preferred_element_type=F32)
             s_band = jnp.where(valid, s_band, MASKED)
-            s_ctx = lax.dot_general(q, k_ctx, across, preferred_element_type=F32) * factor
-            sinks = jnp.where(upper, sink[4 * x + 2 * h], sink[4 * x + 2 * h + 1])
+            s_ctx = lax.dot_general(q, k_ctx, across, preferred_element_type=F32)
+            sinks = jnp.where(upper, sink[4 * x + 2 * h], sink[4 * x + 2 * h + 1]) * to_scores
             top = jnp.maximum(
                 jnp.maximum(jnp.max(s_band, axis=-1, keepdims=True), jnp.max(s_ctx, axis=-1, keepdims=True)), sinks
             )
-            e_band = jnp.exp(s_band - top)
-            e_ctx = jnp.exp(s_ctx - top)
+            e_band = jnp.exp2((s_band - top) * power)
+            e_ctx = jnp.exp2((s_ctx - top) * power)
             total = (
                 jnp.sum(e_band, axis=-1, keepdims=True)
                 + jnp.sum(e_ctx, axis=-1, keepdims=True)
-                + jnp.exp(sinks - top)
+                + jnp.exp2((sinks - top) * power)
             )
             value = jnp.dot(e_band.astype(BF16), v_band, preferred_element_type=F32)
             value += jnp.dot(e_ctx.astype(BF16), v_ctx, preferred_element_type=F32)
@@ -471,35 +468,33 @@
     received(ckv.at[1 - core], cc_r)
     attend(opposite, 3, (1 - core,))
     received(w_out.at[1 - core], wo_r)
-    o_s, d_s = pair()
-    c_s, _ = pair()
+    ring_s = one()
     left_r, right_r = pair()
-    for sem in (o_s, d_s, c_s):
-        drained_at_end(partial.at[0], sem)
+    drained_at_end(partial.at[0:3], ring_s)
     for c in range(PIECES):
         output(3, 1, c * PIECE, PIECE)
         output(3, 1, HALF + c * PIECE, PIECE)
         lower = pl.ds(c * PIECE, PIECE)
         higher = pl.ds(HALF + c * PIECE, PIECE)
-        send(partial.at[3, :, lower], from_left.at[:, lower], o_s, o_r.at[0, c], to_right)
-        send(partial.at[3, :, higher], from_right.at[:, lower], o_s, o_r.at[1, c], to_left)
+        send(partial.at[3, :, lower], from_left.at[:, lower], ring_s, o_r.at[0, c], to_right)
+        send(partial.at[3, :, higher], from_right.at[:, lower], ring_s, o_r.at[1, c], to_left)
     halo_received(opposite != 0, opposite != NX - 1)
     attend(right, 1)
     attend(left, 2)
     for c in range(2 * PIECES):
         output(1, 2, c * PIECE, PIECE)
     low, high = pl.ds(0, HALF), pl.ds(HALF, HALF)
-    send(partial.at[1, :, high], left_done.at[:, high], d_s, left_r, to_right)
-    send(partial.at[2, :, low], right_done.at[:, low], d_s, right_r, to_left)
+    send(partial.at[1, :, high], left_done.at[:, high], ring_s, left_r, to_right)
+    send(partial.at[2, :, low], right_done.at[:, low], ring_s, right_r, to_left)
     for c in range(PIECES):
         lower = pl.ds(c * PIECE, PIECE)
         higher = pl.ds(HALF + c * PIECE, PIECE)
         received(from_left.at[:, lower], o_r.at[0, c])
         partial[1, :, lower] = (partial[1, :, lower].astype(F32) + from_left[:, lower].astype(F32)).astype(BF16)
-        send(partial.at[1, :, lower], left_done.at[:, lower], c_s, left_r, to_right)
+        send(partial.at[1, :, lower], left_done.at[:, lower], ring_s, c_r.at[0, c], to_right)
         received(from_right.at[:, lower], o_r.at[1, c])
         partial[2, :, higher] = (partial[2, :, higher].astype(F32) + from_right[:, lower].astype(F32)).astype(BF16)
-        send(partial.at[2, :, higher], right_done.at[:, higher], c_s, right_r, to_left)
+        send(partial.at[2, :, higher], right_done.at[:, higher], ring_s, c_r.at[1, c], to_left)
     attend(x, 0)
     for c in range(2 * PIECES):
         output(0, 1, c * PIECE, PIECE)
@@ -508,14 +503,14 @@
         for c in range(4):
             at = t * 512 + c * 128
             mod_rows[4:5, at : at + 128] = tg_buf[t, c : c + 1, :]
-    received(left_done, left_r)
-    received(right_done, right_r)
-
-    @pl.loop(0, BLOCK // ROWS)
-    def _(i):
-        at = pl.ds(pl.multiple_of(i * ROWS, ROWS), ROWS)
-        projected = partial[0, at, :].astype(F32) + left_done[at, :].astype(F32) + right_done[at, :].astype(F32)
-        out[at, :] = (x_raw[x, at, :].astype(F32) + mod_rows[4:5, :] * projected).astype(BF16)
+    received(left_done.at[:, high], left_r)
+    received(right_done.at[:, low], right_r)
+    for c in range(PIECES):
+        for half, done in enumerate((left_done, right_done)):
+            at = pl.ds(half * HALF + c * PIECE, PIECE)
+            received(done.at[:, at], c_r.at[half, c])
+            projected = partial[0, :, at].astype(F32) + left_done[:, at].astype(F32) + right_done[:, at].astype(F32)
+            out[:, at] = (x_raw[x, :, at].astype(F32) + mod_rows[4:5, at] * projected).astype(BF16)
 
     for copy in drains:
         copy.wait_send()
@@ -537,8 +532,7 @@
         in_specs=[anywhere] * 13,
         out_specs=inside,
         scratch_shapes=[
-            pltpu.VMEM((NSP, 128), F32),
-            pltpu.VMEM((NSP, 128), F32),
+            pltpu.VMEM((2, NSP, 128), F32),
             pltpu.SMEM((16,), F32),
             pltpu.VMEM((8, 128), F32),
             pltpu.VMEM((NX, BLOCK, HEAD), F32),
@@ -568,7 +562,7 @@
             pltpu.VMEM((BLOCK, HALF), BF16),
             pltpu.VMEM((BLOCK, WIDTH), BF16),
             pltpu.VMEM((BLOCK, WIDTH), BF16),
-            dma((13,)), dma((12,)), dma((7,)), dma((8,)), dma((4,)), dma((2, PIECES)), dma((SINGLE,)),
+            dma((8,)), dma((6,)), dma((3,)), dma((4,)), dma((2, PIECES)), dma((2, PIECES)), dma((SINGLE,)),
         ],
         compiler_params=pltpu.CompilerParams(
             collective_id=0, has_side_effects=True, vmem_limit_bytes=60 * 1024 * 1024

time: 57.1 us -> 56.8 us (level)
  no operation moved by 1% of the time
where the time goes in v4:
time: 56.8 us; the launch traced here: 56.7 us
  Pallas kernels  55.9 us (98%)
  local copies, waits for them, and re-layouts  0.8 us (1%)
    pallas_call x1, Pallas kernels, shards(): pl.pallas_call(kernel, out_shape=pltpu.VMEM((BLOCK, WIDTH), BF16), in_spe...  55.9 us

profile of v4, /device:TPU:1, one launch (start us, length us, event | category | flops | bytes accessed | tf_op | source)
XLA Modules:
  0.0 56.7 jit_solution(8400440618511509562)
XLA Ops:
  0.0 55.9 %shard_map.127 = bf16[64,4096]{1,0:T(8,128)(2,1)S(1)} custom-call(bf16[64,4096]{1,0:T(8,128)(2,1)} %latent.1, bf16[32,4096]{1,0:T(8,128)(2,1)} %context.1, f32[32,128]{1,0:T(8,128)} %bitcast.2, f32[32,128]{1,0:T(8,128)} %bitcast.3, bf16[128,512]{1,0:T(8,128)(2,1)} %w_shift.1, bf16[128,512]{1,0:T(8,128)(2,1)} %w_scale.1, bf16[128,512]{1,0:T(8,128)(2,1)} %w_gate.1, ...), custom_call_target="tpu_custom_call" | custom-call | tf_op jit(solution)/shard_map/pallas_call | solution.py:529
  55.9 0.8 %copy.15 = bf16[64,4096]{1,0:T(8,128)(2,1)} copy(bf16[64,4096]{1,0:T(8,128)(2,1)S(1)} %shard_map.127) | data formatting | bytes 1048576

commit v5 on v4

--- a/solution.py
+++ b/solution.py
@@ -380,12 +380,13 @@
 
     for slot in range(3):
         share(slot)
-    halo_when(opposite != NX - 1, opposite != 0)
+    halo_when(x == 2, x == 1)
     project(0, 0, 3)
 
     received(ckv.at[core, 0, 0:7], cz_r)
     for d in (3, 5, 4, 1, 7, 2, 6):
         spread(d)
+    halo_when((x == 0) | (x == NX - 1), (x == 0) | (x == NX - 1))
     @pl.loop(0, 3)
     def _(slot):
         turn_queries(slot)

time: 56.8 us -> 56.7 us (level)
  no operation moved by 1% of the time
where the time goes in v5:
time: 56.7 us; the launch traced here: 56.6 us
  Pallas kernels  55.8 us (98%)
  local copies, waits for them, and re-layouts  0.8 us (1%)
    pallas_call x1, Pallas kernels, shards(): pl.pallas_call(kernel, out_shape=pltpu.VMEM((BLOCK, WIDTH), BF16), in_spe...  55.8 us

profile of v5, /device:TPU:1, one launch (start us, length us, event | category | flops | bytes accessed | tf_op | source)
XLA Modules:
  0.0 56.6 jit_solution(16890846654781377675)
XLA Ops:
  0.0 55.8 %shard_map.127 = bf16[64,4096]{1,0:T(8,128)(2,1)S(1)} custom-call(bf16[64,4096]{1,0:T(8,128)(2,1)} %latent.1, bf16[32,4096]{1,0:T(8,128)(2,1)} %context.1, f32[32,128]{1,0:T(8,128)} %bitcast.2, f32[32,128]{1,0:T(8,128)} %bitcast.3, bf16[128,512]{1,0:T(8,128)(2,1)} %w_shift.1, bf16[128,512]{1,0:T(8,128)(2,1)} %w_scale.1, bf16[128,512]{1,0:T(8,128)(2,1)} %w_gate.1, ...), custom_call_target="tpu_custom_call" | custom-call | tf_op jit(solution)/shard_map/pallas_call | solution.py:530
  55.8 0.8 %copy.15 = bf16[64,4096]{1,0:T(8,128)(2,1)} copy(bf16[64,4096]{1,0:T(8,128)(2,1)S(1)} %shard_map.127) | data formatting | bytes 1048576
